TPU v7x, 32 devices: a whole 2x2x4 slice. The times are simulated.
32 devices in a mesh: ep: 8 (over z, x), tp: 4 (over y, core).
Axes of the slice: x: 2, y: 2, z: 4, core: 2. Of those that a mesh axis runs over, the one named last changes fastest.
Arguments:
- conv_value: bfloat16 [8192, 1024], P('ep', 'tp'), may hold values from -600 to 600
- conv_gate: bfloat16 [8192, 1024], P('ep', 'tp'), may hold values from -8 to 8
- depth_weight: float32 [31, 1024], replicated, may hold values from -1 to 1
- norm_gain: float32 [1024], replicated, may hold values from 0.1 to 1.9
- norm_shift: float32 [1024], replicated, may hold values from -3 to 3
- conv_out_weight: bfloat16 [1024, 2048], P('tp'), may hold values from -0.1875 to 0.1875
- moe_input: bfloat16 [12288, 2048], P(('ep', 'tp')), may hold values from -6 to 6
- moe_gain: float32 [2048], replicated, may hold values from 0.1 to 1.9
- route_experts: int32 [12288, 2], P(('ep', 'tp')), may hold values from 0 to 7, as said below
- route_scores: float32 [12288, 2], P(('ep', 'tp')), may hold values from -8 to 8
- expert_gate: bfloat16 [8, 2048, 512], P('ep'), may hold values from -0.125 to 0.125
- expert_up: bfloat16 [8, 2048, 512], P('ep'), may hold values from -0.125 to 0.125
- expert_down: bfloat16 [8, 512, 2048], P('ep'), may hold values from -1 to 1
Outputs:
- conv_out: bfloat16 [8192, 2048], P(('ep', 'tp'))
- moe_out: bfloat16 [12288, 2048], P(('ep', 'tp'))
Inputs may be any that keep to these rules, and one draw needn't show every extreme that they name: `route_experts`: each row names two different experts that lie in one group of 2 consecutive experts.
All inputs are finite; a program needn't handle non-finite values.
Results may differ from a plain program's by a relative error of at most 0.009.
Values may be sent and summed in bfloat16 or wider, within the bound.
A program may use at most 128 MiB of HBM per device.

v0:
```python
import jax
import jax.numpy as jnp
from jax import lax
from jax.sharding import PartitionSpec as P

GROUPS = 4
TOP = 2


def passed_along(x, axis, by):
    peers = lax.axis_size(axis)
    pairs = [(i, i + by) for i in range(peers) if 0 <= i + by < peers]
    return lax.ppermute(x, axis, pairs)


def gated_rows(value, gate):
    return (value.astype(jnp.float32) * jax.nn.sigmoid(gate.astype(jnp.float32))).astype(
        jnp.bfloat16
    )


def conv_half(conv_value, conv_gate, earlier, depth_weight, norm_gain, norm_shift, conv_out_weight):
    channels = conv_value.shape[1]
    length = conv_value.shape[0]
    first_col = lax.axis_index("tp") * channels
    taps = lax.dynamic_slice_in_dim(depth_weight, first_col, channels, 1)
    gains = lax.dynamic_slice_in_dim(norm_gain, first_col, channels, 0)
    shifts = lax.dynamic_slice_in_dim(norm_shift, first_col, channels, 0)
    reach = taps.shape[0] - 1
    gated = gated_rows(conv_value, conv_gate)
    padded = jnp.concatenate([earlier, gated], 0).astype(jnp.float32)
    filtered = taps[0] * padded[0:length]
    for offset in range(1, reach + 1):
        filtered = filtered + taps[offset] * padded[offset : offset + length]
    sums, squares = lax.psum(
        (jnp.sum(filtered, axis=1), jnp.sum(filtered * filtered, axis=1)), "tp"
    )
    all_channels = channels * lax.axis_size("tp")
    center = (sums / all_channels)[:, None]
    spread = (squares / all_channels)[:, None] - center * center
    normed = (filtered - center) * lax.rsqrt(spread + 1e-05) * gains + shifts
    activated = jax.nn.silu(normed).astype(jnp.bfloat16)
    partial_value = jnp.dot(activated, conv_out_weight, preferred_element_type=jnp.float32)
    return partial_value.astype(jnp.bfloat16)


def scattered_sum(partial):
    peers = lax.axis_size("tp")
    me = lax.axis_index("tp")
    size = partial.shape[0] // peers
    total = lax.dynamic_slice_in_dim(partial, me * size, size, 0).astype(jnp.float32)
    for mask in range(peers - 1, 0, -1):
        block = lax.dynamic_slice_in_dim(partial, (me ^ mask) * size, size, 0)
        total = total + swapped(block, "tp", mask).astype(jnp.float32)
    return total.astype(jnp.bfloat16)


def moe_half(moe_input, moe_gain, route_experts, route_scores, expert_gate, expert_up, expert_down):
    rows = moe_input.shape[0]
    model_width = moe_input.shape[1]
    experts_all = lax.axis_size("ep")
    capacity = 2 * (3 * TOP * rows // (4 * experts_all))
    widened = moe_input.astype(jnp.float32)
    normal_in = (
        widened * lax.rsqrt(jnp.mean(widened * widened, axis=-1, keepdims=True) + 1e-06) * moe_gain
    ).astype(jnp.bfloat16)
    chosen = route_experts.reshape(-1)
    onehot = (chosen[:, None] == jnp.arange(experts_all, dtype=jnp.int32)[None, :]).astype(
        jnp.int32
    )
    slot_rank = jnp.sum(jnp.cumsum(onehot, axis=0) * onehot, axis=-1) - 1
    slot_index = jnp.where(
        slot_rank < capacity, chosen * capacity + slot_rank, experts_all * capacity
    )
    source_row = jnp.arange(rows * TOP, dtype=jnp.int32) // TOP
    slot_token = (
        jnp.full((experts_all * capacity,), rows, jnp.int32)
        .at[slot_index]
        .set(source_row, mode="drop")
    )
    padded_in = jnp.concatenate([normal_in, jnp.zeros((1, model_width), jnp.bfloat16)], 0)
    send_buffer = padded_in[slot_token].reshape(experts_all, capacity, model_width)
    arrived = lax.all_to_all(send_buffer, "ep", split_axis=0, concat_axis=0, tiled=True)
    flat_rows = arrived.reshape(-1, model_width)
    gate_act = jnp.dot(flat_rows, expert_gate[0], preferred_element_type=jnp.float32)
    up_act = jnp.dot(flat_rows, expert_up[0], preferred_element_type=jnp.float32)
    inner = (jax.nn.silu(gate_act) * up_act).astype(jnp.bfloat16)
    result = jnp.dot(inner, expert_down[0], preferred_element_type=jnp.float32).astype(jnp.bfloat16)
    returned = lax.all_to_all(
        result.reshape(arrived.shape), "ep", split_axis=0, concat_axis=0, tiled=True
    )
    returned_flat = jnp.concatenate(
        [
            returned.reshape(experts_all * capacity, model_width),
            jnp.zeros((1, model_width), jnp.bfloat16),
        ],
        0,
    )
    picked = returned_flat[slot_index].reshape(rows, TOP, model_width)
    group_gate = jax.nn.sigmoid(route_scores[:, 0])
    first_weight = (group_gate * jax.nn.sigmoid(route_scores[:, 1]))[:, None]
    second_weight = (group_gate * jax.nn.sigmoid(-route_scores[:, 1]))[:, None]
    combined = first_weight * picked[:, 0].astype(jnp.float32) + second_weight * picked[
        :, 1
    ].astype(jnp.float32)
    return combined.astype(jnp.bfloat16)


def swapped(x, axis, mask):
    peers = lax.axis_size(axis)
    return lax.ppermute(x, axis, [(i, i ^ mask) for i in range(peers)])


def partner_weights(expert_gate, expert_up, expert_down, place):
    peers = lax.axis_size("tp")
    share = expert_down.shape[1] // peers
    first = place * share
    gate_up = jnp.concatenate(
        [
            lax.dynamic_slice_in_dim(expert_gate[0], first, share, 1),
            lax.dynamic_slice_in_dim(expert_up[0], first, share, 1),
        ],
        1,
    )
    down = lax.dynamic_slice_in_dim(expert_down[0], first, share, 0)
    gate_ups = [swapped(gate_up, "ep", 1)]
    downs = [swapped(down, "ep", 1)]
    mask = peers // 2
    while mask:
        gate_ups = gate_ups + [swapped(piece, "tp", mask) for piece in gate_ups]
        downs = downs + [swapped(piece, "tp", mask) for piece in downs]
        mask //= 2
    gate = jnp.concatenate([piece[:, :share] for piece in gate_ups], 1)
    up = jnp.concatenate([piece[:, share:] for piece in gate_ups], 1)
    return gate, up, jnp.concatenate(downs, 0)


def one_expert(rows, gate, up, down):
    gate_act = jnp.dot(rows, gate, preferred_element_type=jnp.float32)
    up_act = jnp.dot(rows, up, preferred_element_type=jnp.float32)
    inner = (jax.nn.silu(gate_act) * up_act).astype(jnp.bfloat16)
    return jnp.dot(inner, down, preferred_element_type=jnp.float32).astype(jnp.bfloat16)


def pair_half(moe_input, moe_gain, route_experts, route_scores, expert_gate, expert_up, expert_down, first, beside):
    rows, model_width = moe_input.shape
    experts_all = lax.axis_size("ep")
    groups = experts_all // TOP
    capacity = 2 * (3 * TOP * rows // (4 * experts_all))
    widened = moe_input.astype(jnp.float32)
    normal_in = (
        widened * lax.rsqrt(jnp.mean(widened * widened, axis=-1, keepdims=True) + 1e-06) * moe_gain
    ).astype(jnp.bfloat16)
    row_group = route_experts[:, 0] // TOP
    onehot = (row_group[:, None] == jnp.arange(groups, dtype=jnp.int32)[None, :]).astype(
        jnp.bfloat16
    )
    order = jnp.arange(rows, dtype=jnp.int32)
    before = (order[:, None] > order[None, :]).astype(jnp.bfloat16)
    ranks = jnp.dot(before, onehot, preferred_element_type=jnp.float32)
    rank = jnp.sum(ranks * onehot.astype(jnp.float32), axis=1).astype(jnp.int32)
    slot = jnp.where(rank < capacity, row_group * capacity + rank, -1)
    slots = jnp.arange(groups * capacity, dtype=jnp.int32)
    pick = (slots[:, None] == slot[None, :]).astype(jnp.bfloat16)
    group_gate = jax.nn.sigmoid(route_scores[:, 0])
    first_weight = group_gate * jax.nn.sigmoid(route_scores[:, 1])
    second_weight = group_gate * jax.nn.sigmoid(-route_scores[:, 1])
    in_order = route_experts[:, 0] % TOP == 0
    low_weight = jnp.where(in_order, first_weight, second_weight)
    high_weight = jnp.where(in_order, second_weight, first_weight)
    lane = jnp.arange(128, dtype=jnp.int32)[None, :]
    weights = jnp.where(lane < 64, low_weight[:, None], high_weight[:, None])
    coarse = lax.reduce_precision(weights, 8, 7)
    extra = jnp.where(lane % 64 < 32, coarse, weights - coarse).astype(jnp.bfloat16)
    sent = jnp.dot(
        pick, jnp.concatenate([normal_in, extra], 1), preferred_element_type=jnp.float32
    ).astype(jnp.bfloat16)
    sent, _, place = lax.optimization_barrier((sent, first, lax.axis_index("tp")))
    other = partner_weights(expert_gate, expert_up, expert_down, place)
    along = [[TOP * g + x for g in range(groups)] for x in range(TOP)]
    arrived = lax.all_to_all(
        sent.reshape(groups, capacity, -1),
        "ep",
        split_axis=0,
        concat_axis=0,
        axis_index_groups=along,
        tiled=True,
    ).reshape(groups * capacity, -1)
    arrived, beside = lax.optimization_barrier((arrived, beside))
    flat_rows = arrived[:, :model_width]
    tail = arrived[:, model_width:].astype(jnp.float32)
    low = tail[:, 0:1] + tail[:, 32:33]
    high = tail[:, 64:65] + tail[:, 96:97]
    even = lax.axis_index("ep") % TOP == 0
    mine = one_expert(flat_rows, expert_gate[0], expert_up[0], expert_down[0])
    theirs = one_expert(flat_rows, *other)
    combined = jnp.where(even, low, high) * mine.astype(jnp.float32) + jnp.where(
        even, high, low
    ) * theirs.astype(jnp.float32)
    returned = lax.all_to_all(
        combined.astype(jnp.bfloat16).reshape(groups, capacity, model_width),
        "ep",
        split_axis=0,
        concat_axis=0,
        axis_index_groups=along,
        tiled=True,
    ).reshape(groups * capacity, model_width)
    put = (slot[:, None] == slots[None, :]).astype(jnp.bfloat16)
    moe_out = jnp.dot(put, returned, preferred_element_type=jnp.float32).astype(jnp.bfloat16)
    return moe_out, beside


def on_device(
    conv_value,
    conv_gate,
    depth_weight,
    norm_gain,
    norm_shift,
    conv_out_weight,
    moe_input,
    moe_gain,
    route_experts,
    route_scores,
    expert_gate,
    expert_up,
    expert_down,
):
    last = conv_value.shape[0] - depth_weight.shape[0] + 1
    earlier = passed_along(gated_rows(conv_value[last:], conv_gate[last:]), "ep", 1)
    partial = conv_half(
        conv_value, conv_gate, earlier, depth_weight, norm_gain, norm_shift, conv_out_weight
    )
    moe_args = (
        moe_input, moe_gain, route_experts, route_scores, expert_gate, expert_up, expert_down
    )
    if lax.axis_size("ep") // GROUPS == TOP:
        moe_out, partial = pair_half(*moe_args, earlier, partial)
    else:
        moe_out = moe_half(*moe_args)
    return (scattered_sum(partial), moe_out)


def solution(mesh):
    in_specs = (
        P("ep", "tp"),
        P("ep", "tp"),
        P(),
        P(),
        P(),
        P("tp", None),
        P(("ep", "tp"), None),
        P(),
        P(("ep", "tp"), None),
        P(("ep", "tp"), None),
        P("ep", None, None),
        P("ep", None, None),
        P("ep", None, None),
    )
    out_specs = (P(("ep", "tp"), None), P(("ep", "tp"), None))
    return jax.shard_map(
        on_device, mesh=mesh, in_specs=in_specs, out_specs=out_specs, check_vma=False
    )
```

profile of v0, /device:TPU:8, one launch (start us, length us, event | category | flops | bytes accessed | tf_op | source)
XLA Modules:
  0.0 172.3 jit_solution(7208101400824003886)
XLA Ops:
  1.6 3.5 %collective-permute-start = (bf16[30,256]{1,0:T(8,128)(2,1)S(1)}, bf16[30,256]{1,0:T(8,128)(2,1)S(1)}, u32[]{:S(2)}, u32[]{:S(2)}) collective-permute-start(bf16[30,256]{1,0:T(8,128)(2,1)S(1)} %multiply_convert_fusion.5), channel_id=1, source_target_pairs={{0,4},{4,8},{8,12},{12,16},{16,20},{20,24},{24,28},{1,5},{5,9},{9,... | collective-permute-start | bytes 46088 | tf_op jit(solution)/shard_map/ppermute | solution.py:13
  6.8 1.8 %fusion = f32[384]{0:T(512)S(1)} fusion(bf16[384,2048]{1,0:T(8,128)(2,1)} %param.19), kind=kLoop, calls=%fused_computation.5 | loop fusion | flops 2358912 | bytes 1574400 | tf_op jit(solution)/shard_map/reduce_sum | solution.py:152
  8.7 1.1 fusion.2
  10.0 3.0 %convolution_convert_fusion = bf16[576,2176]{1,0:T(8,128)(2,1)} fusion(bf16[384,128]{1,0:T(8,128)(2,1)S(1)} %fusion.92, bf16[384,2048]{1,0:T(8,128)(2,1)S(1)} %fusion.2, s32[384]{0:T(512)S(1)} %fusion.98), kind=kOutput, calls=%fused_computation.1 | convolution fusion | flops 967409664 | bytes 4179456 | tf_op jit(solution)/shard_map/dot_general | solution.py:175
  13.1 1.1 dynamic-slice_bitcast_fusion.1
  14.2 1.1 dynamic-slice_bitcast_fusion.2
  15.3 1.1 pad_maximum_fusion
  16.4 1.5 collective-permute-start.4
  19.4 1.1 fusion.118
  20.6 1.3 constant_dynamic-slice_fusion
  21.9 1.4 multiply_convert_fusion.2
  23.2 4.9 %all-to-all-start = ((bf16[4,144,2176]{2,1,0:T(8,128)(2,1)}), bf16[4,144,2176]{2,1,0:T(8,128)(2,1)}, u32[]{:S(2)}, u32[]{:S(2)}) async-start(bf16[4,144,2176]{2,1,0:T(8,128)(2,1)} %bitcast.58), calls=%async_computation | async-start | bytes 5013504 | tf_op jit(solution)/shard_map/all_to_all | solution.py:181
  30.0 12.7 %collective-permute-done.4 = bf16[2048,256]{1,0:T(8,128)(2,1)} collective-permute-done((bf16[2048,256]{1,0:T(8,128)(2,1)}, bf16[2048,256]{1,0:T(8,128)(2,1)}, u32[]{:S(2)}, u32[]{:S(2)}) %collective-permute-start.4) | collective-permute-done | bytes 1048608 | tf_op jit(solution)/shard_map/ppermute | solution.py:111
  42.7 1.5 collective-permute-start.5
  44.2 4.4 %fusion.111 = (f32[1024]{0:T(1024)S(1)}, f32[1024]{0:T(1024)S(1)}, f32[1024,256]{1,0:T(8,128)S(1)}) fusion(f32[1054,256]{1,0:T(8,128)S(1)} %maximum_convert_fusion, f32[256]{0:T(256)S(1)} %bitcast.72, f32[256]{0:T(256)S(1)} %bitcast.74, f32[256]{0:T(256)S(1)} %bitcast.75, f32[256]{0:T(256)S(1)} %bitcast.76, f32[256]{0:T(256)S(1)} %bitcast.77, ...), kind=kLoop, calls=%fused_computation.186 | loop fusion | flops 16775168 | bytes 33594368 | tf_op jit(solution)/shard_map/reduce_sum | solution.py:36
  48.7 19.7 %all-reduce = (f32[1024]{0:T(1024)S(1)}, f32[1024]{0:T(1024)S(1)}) all-reduce(f32[1024]{0:T(1024)S(1)} %get-tuple-element.11, f32[1024]{0:T(1024)S(1)} %get-tuple-element.10), channel_id=1, replica_groups=mesh['ep'=8,'tp'=4] {'tp'}, use_global_device_ids=true, to_apply=%region_5.6 | all-reduce | flops 2048 | bytes 16384 | tf_op jit(solution)/shard_map/psum | solution.py:35
  69.0 4.6 %convolution_convert_fusion.1 = bf16[1024,2048]{1,0:T(8,128)(2,1)} fusion(bf16[256,2048]{1,0:T(8,128)(2,1)} %param.18, f32[1024,256]{1,0:T(8,128)S(1)} %get-tuple-element.18, f32[256]{0:T(256)S(1)} %dynamic_slice.38, f32[256]{0:T(256)S(1)} %dynamic_slice.37, f32[1024]{0:T(1024)S(1)} %get-tuple-element.67, f32[1024]{0:T(1024)S(1)} %get-tuple-element.66), kind=kOutput, calls=%fused_computation.4 | convolution fusion | flops 1078198272 | bytes 6301696 | tf_op jit(solution)/shard_map/dot_general | solution.py:43
  74.1 1.3 fusion.114
  75.3 5.6 %collective-permute-done.9 = bf16[128,2048]{1,0:T(8,128)(2,1)} collective-permute-done((bf16[128,2048]{1,0:T(8,128)(2,1)}, bf16[128,2048]{1,0:T(8,128)(2,1)}, u32[]{:S(2)}, u32[]{:S(2)}) %collective-permute-start.9) | collective-permute-done | bytes 524320 | tf_op jit(solution)/shard_map/ppermute | solution.py:111
  80.9 2.3 %fusion.115 = (bf16[2048,128]{1,0:T(8,128)(2,1)}, bf16[2048,128]{1,0:T(8,128)(2,1)}) fusion(bf16[2048,256]{1,0:T(8,128)(2,1)} %collective-permute-done.5), kind=kLoop, calls=%fused_computation.189 | loop fusion | bytes 2097152 | tf_op jit(solution)/shard_map/slice | solution.py:133
  85.3 4.7 %fusion.29 = f32[576,512]{1,0:T(8,128)} fusion(bf16[1,2048,512]{2,1,0:T(8,128)(2,1)} %param.23, bf16[576,2176]{1,0:T(8,128)(2,1)} %bitcast.1), kind=kOutput, calls=%fused_computation.37 | convolution fusion | flops 1207959552 | bytes 5636096 | tf_op jit(solution)/shard_map/dot_general | solution.py:139
  90.9 6.8 %convolution_convert_fusion.3 = bf16[576,2048]{1,0:T(8,128)(2,1)} fusion(bf16[1,512,2048]{2,1,0:T(8,128)(2,1)S(1)} %copy-done, bf16[1,2048,512]{2,1,0:T(8,128)(2,1)} %param.24, bf16[576,2176]{1,0:T(8,128)(2,1)} %bitcast.1, f32[576,512]{1,0:T(8,128)} %fusion.29), kind=kOutput, calls=%fused_computation.9 | convolution fusion | flops 2418868224 | bytes 10092544 | tf_op jit(solution)/shard_map/dot_general | solution.py:142
  98.2 3.6 %fusion.3 = f32[576,512]{1,0:T(8,128)S(1)} fusion(bf16[2048,128]{1,0:T(8,128)(2,1)} %get-tuple-element.33, bf16[2048,128]{1,0:T(8,128)(2,1)} %get-tuple-element.31, bf16[2048,128]{1,0:T(8,128)(2,1)} %get-tuple-element.29, bf16[2048,128]{1,0:T(8,128)(2,1)S(1)} %get-tuple-element.27, bf16[576,2176]{1,0:T(8,128)(2,1)} %bitcast.1), kind=kOutput, calls=%fused_computation.11 | convolution fusion | flops 1216348160 | bytes 5636096 | tf_op jit(solution)/shard_map/dot_general | solution.py:139
  101.8 3.2 %fusion.11 = f32[576,512]{1,0:T(8,128)S(1)} fusion(bf16[2048,128]{1,0:T(8,128)(2,1)S(1)} %copy-done.5, bf16[2048,128]{1,0:T(8,128)(2,1)S(1)} %copy-done.4, bf16[2048,128]{1,0:T(8,128)(2,1)S(1)} %copy-done.3, bf16[2048,128]{1,0:T(8,128)(2,1)S(1)} %get-tuple-element.28, bf16[576,2176]{1,0:T(8,128)(2,1)} %bitcast.1), kind=kOutput, calls=%fused_computation.19 | convolution fusion | flops 1216348160 | bytes 5636096 | tf_op jit(solution)/shard_map/dot_general | solution.py:140
  105.1 4.6 %add_convert_fusion = bf16[576,2048]{1,0:T(8,128)(2,1)} fusion(bf16[576,2048]{1,0:T(8,128)(2,1)S(1)} %copy-done.7, f32[576]{0:T(1024)S(1)} %get-tuple-element.13, f32[576]{0:T(1024)S(1)} %get-tuple-element.12, bf16[128,2048]{1,0:T(8,128)(2,1)} %collective-permute-done.11, bf16[128,2048]{1,0:T(8,128)(2,1)} %collective-permute-done.10, ...), kind=kOutput, calls=%fused_computation | convolution fusion | flops 1226375168 | bytes 9179648 | tf_op jit(solution)/shard_map/dot_general | solution.py:142
  109.6 5.2 %all-to-all-start.1 = ((bf16[4,144,2048]{2,1,0:T(8,128)(2,1)}), bf16[4,144,2048]{2,1,0:T(8,128)(2,1)}, u32[]{:S(2)}, u32[]{:S(2)}) async-start(bf16[4,144,2048]{2,1,0:T(8,128)(2,1)} %bitcast.59), calls=%async_computation.1 | async-start | bytes 4718592 | tf_op jit(solution)/shard_map/all_to_all | solution.py:200
  114.9 2.2 %constant_dynamic-slice_fusion.3 = (bf16[256,2048]{1,0:T(8,128)(2,1)S(1)}, bf16[256,2048]{1,0:T(8,128)(2,1)S(1)}, bf16[256,2048]{1,0:T(8,128)(2,1)S(1)}) fusion(bf16[1024,2048]{1,0:T(8,128)(2,1)} %convolution_convert_fusion.1, s32[]{:T(128)S(6)} %select_n.109, s32[]{:T(128)S(6)} %select_n.111, s32[]{:T(128)S(6)} %select_n.110), kind=kLoop, calls=%fused_computation.167 | loop fusion | bytes 6291468 | tf_op jit(solution)/shard_map/dynamic_slice | solution.py:53
  117.1 1.1 collective-permute-start.1
  119.1 23.4 %collective-permute-done.1 = bf16[256,2048]{1,0:T(8,128)(2,1)S(1)} collective-permute-done((bf16[256,2048]{1,0:T(8,128)(2,1)S(1)}, bf16[256,2048]{1,0:T(8,128)(2,1)S(1)}, u32[]{:S(2)}, u32[]{:S(2)}) %collective-permute-start.1) | collective-permute-done | bytes 1048608 | tf_op jit(solution)/shard_map/ppermute | solution.py:111
  142.5 22.6 %collective-permute-done.2 = bf16[256,2048]{1,0:T(8,128)(2,1)S(1)} collective-permute-done((bf16[256,2048]{1,0:T(8,128)(2,1)S(1)}, bf16[256,2048]{1,0:T(8,128)(2,1)S(1)}, u32[]{:S(2)}, u32[]{:S(2)}) %collective-permute-start.2) | collective-permute-done | bytes 1048608 | tf_op jit(solution)/shard_map/ppermute | solution.py:111
  165.1 2.9 %add_convert_fusion.1 = bf16[256,2048]{1,0:T(8,128)(2,1)} fusion(bf16[256,2048]{1,0:T(8,128)(2,1)S(1)} %collective-permute-done.3, bf16[256,2048]{1,0:T(8,128)(2,1)S(1)} %collective-permute-done.2, bf16[256,2048]{1,0:T(8,128)(2,1)S(1)} %collective-permute-done.1, bf16[1024,2048]{1,0:T(8,128)(2,1)} %convolution_convert_fusion.1, s32[]{:T(128)S(6)} %select_n.108), kind=kLoop, calls=%fused_computation.39 | loop fusion | flops 4194304 | bytes 5242884 | tf_op jit(solution)/shard_map/convert_element_type | solution.py:55
  168.0 4.2 %convolution_convert_fusion.4 = bf16[384,2048]{1,0:T(8,128)(2,1)} fusion(bf16[576,2048]{1,0:T(8,128)(2,1)} %bitcast.40, s32[384]{0:T(512)S(1)} %fusion.102), kind=kOutput, calls=%fused_computation.10 | convolution fusion | flops 906977280 | bytes 3933696 | tf_op jit(solution)/shard_map/dot_general | solution.py:209
  (54 shorter events, 11.7 us)
Async XLA Ops:
  0.6 27.5 %copy-start = (bf16[1,512,2048]{2,1,0:T(8,128)(2,1)S(1)}, bf16[1,512,2048]{2,1,0:T(8,128)(2,1)}, u32[]{:S(2)}) copy-start(bf16[1,512,2048]{2,1,0:T(8,128)(2,1)} %param.25) | copy-start | bytes 6291460
  0.6 8.0 %copy-start.1 = (bf16[384,2048]{1,0:T(8,128)(2,1)S(1)}, bf16[384,2048]{1,0:T(8,128)(2,1)}, u32[]{:S(2)}) copy-start(bf16[384,2048]{1,0:T(8,128)(2,1)} %param.19) | copy-start | bytes 4718596
  1.6 11.5 %collective-permute-start = (bf16[30,256]{1,0:T(8,128)(2,1)S(1)}, bf16[30,256]{1,0:T(8,128)(2,1)S(1)}, u32[]{:S(2)}, u32[]{:S(2)}) collective-permute-start(bf16[30,256]{1,0:T(8,128)(2,1)S(1)} %multiply_convert_fusion.5), channel_id=1, source_target_pairs={{0,4},{4,8},{8,12},{12,16},{16,20},{20,24},{24,28},{1,5},{5,9},{9,... | collective-permute-start | bytes 46088 | tf_op jit(solution)/shard_map/ppermute | solution.py:13
  6.8 3.0 %copy-start.6 = (f32[384,2]{0,1:T(2,128)S(1)}, f32[384,2]{0,1:T(2,128)}, u32[]{:S(2)}) copy-start(f32[384,2]{0,1:T(2,128)} %param.22) | copy-start | bytes 9220
  13.1 8.8 %copy-start.2 = (bf16[1024,256]{1,0:T(8,128)(2,1)S(1)}, bf16[1024,256]{1,0:T(8,128)(2,1)}, u32[]{:S(2)}) copy-start(bf16[1024,256]{1,0:T(8,128)(2,1)} %param.14) | copy-start | bytes 1572868
  16.4 26.3 %collective-permute-start.4 = (bf16[2048,256]{1,0:T(8,128)(2,1)}, bf16[2048,256]{1,0:T(8,128)(2,1)}, u32[]{:S(2)}, u32[]{:S(2)}) collective-permute-start(bf16[2048,256]{1,0:T(8,128)(2,1)} %pad_maximum_fusion), channel_id=1, source_target_pairs={{0,4},{4,0},{8,12},{12,8},{16,20},{20,16},{24,28},{28,24},{1,5},{5... | collective-permute-start | bytes 3145736 | tf_op jit(solution)/shard_map/ppermute | solution.py:111
  23.2 62.1 %all-to-all-start = ((bf16[4,144,2176]{2,1,0:T(8,128)(2,1)}), bf16[4,144,2176]{2,1,0:T(8,128)(2,1)}, u32[]{:S(2)}, u32[]{:S(2)}) async-start(bf16[4,144,2176]{2,1,0:T(8,128)(2,1)} %bitcast.58), calls=%async_computation | async-start | bytes 5013504 | tf_op jit(solution)/shard_map/all_to_all | solution.py:181
  29.0 39.4 %collective-permute-start.8 = (bf16[128,2048]{1,0:T(8,128)(2,1)}, bf16[128,2048]{1,0:T(8,128)(2,1)}, u32[]{:S(2)}, u32[]{:S(2)}) collective-permute-start(bf16[128,2048]{1,0:T(8,128)(2,1)} %dynamic-slice_bitcast_fusion), channel_id=1, source_target_pairs={{0,4},{4,0},{8,12},{12,8},{16,20},{20,16},{24,28},{28,24},{1,5},{5... | collective-permute-start | bytes 1572872 | tf_op jit(solution)/shard_map/ppermute | solution.py:111
  42.7 31.3 %collective-permute-start.5 = (bf16[2048,256]{1,0:T(8,128)(2,1)}, bf16[2048,256]{1,0:T(8,128)(2,1)}, u32[]{:S(2)}, u32[]{:S(2)}) collective-permute-start(bf16[2048,256]{1,0:T(8,128)(2,1)} %collective-permute-done.4), channel_id=1, source_target_pairs={{0,2},{1,3},{2,0},{3,1},{4,6},{5,7},{6,4},{7,5},{8,10},{9,11},{10,... | collective-permute-start | bytes 3145736 | tf_op jit(solution)/shard_map/ppermute | solution.py:111
  68.4 12.5 %collective-permute-start.9 = (bf16[128,2048]{1,0:T(8,128)(2,1)}, bf16[128,2048]{1,0:T(8,128)(2,1)}, u32[]{:S(2)}, u32[]{:S(2)}) collective-permute-start(bf16[128,2048]{1,0:T(8,128)(2,1)} %collective-permute-done.8), channel_id=1, source_target_pairs={{0,2},{1,3},{2,0},{3,1},{4,6},{5,7},{6,4},{7,5},{8,10},{9,11},{10,... | collective-permute-start | bytes 1572872 | tf_op jit(solution)/shard_map/ppermute | solution.py:111
  69.0 14.2 %collective-permute-start.6 = (bf16[2048,256]{1,0:T(8,128)(2,1)}, bf16[2048,256]{1,0:T(8,128)(2,1)S(1)}, u32[]{:S(2)}, u32[]{:S(2)}) collective-permute-start(bf16[2048,256]{1,0:T(8,128)(2,1)} %collective-permute-done.4), channel_id=1, source_target_pairs={{0,1},{1,0},{2,3},{3,2},{4,5},{5,4},{6,7},{7,6},{8,9},{9,8},{10,11... | collective-permute-start | bytes 3145736 | tf_op jit(solution)/shard_map/ppermute | solution.py:111
  73.5 31.5 %collective-permute-start.10 = (bf16[128,2048]{1,0:T(8,128)(2,1)}, bf16[128,2048]{1,0:T(8,128)(2,1)}, u32[]{:S(2)}, u32[]{:S(2)}) collective-permute-start(bf16[128,2048]{1,0:T(8,128)(2,1)} %collective-permute-done.8), channel_id=1, source_target_pairs={{0,1},{1,0},{2,3},{3,2},{4,5},{5,4},{6,7},{7,6},{8,9},{9,8},{10,11... | collective-permute-start | bytes 1572872 | tf_op jit(solution)/shard_map/ppermute | solution.py:111
  74.1 10.2 %collective-permute-start.7 = (bf16[2048,256]{1,0:T(8,128)(2,1)}, bf16[2048,256]{1,0:T(8,128)(2,1)S(1)}, u32[]{:S(2)}, u32[]{:S(2)}) collective-permute-start(bf16[2048,256]{1,0:T(8,128)(2,1)} %collective-permute-done.5), channel_id=1, source_target_pairs={{0,1},{1,0},{2,3},{3,2},{4,5},{5,4},{6,7},{7,6},{8,9},{9,8},{10,11... | collective-permute-start | bytes 3145736 | tf_op jit(solution)/shard_map/ppermute | solution.py:111
  80.9 24.1 %collective-permute-start.11 = (bf16[128,2048]{1,0:T(8,128)(2,1)}, bf16[128,2048]{1,0:T(8,128)(2,1)}, u32[]{:S(2)}, u32[]{:S(2)}) collective-permute-start(bf16[128,2048]{1,0:T(8,128)(2,1)} %collective-permute-done.9), channel_id=1, source_target_pairs={{0,1},{1,0},{2,3},{3,2},{4,5},{5,4},{6,7},{7,6},{8,9},{9,8},{10,11... | collective-permute-start | bytes 1572872 | tf_op jit(solution)/shard_map/ppermute | solution.py:111
  98.2 3.6 %copy-start.3 = (bf16[2048,128]{1,0:T(8,128)(2,1)S(1)}, bf16[2048,128]{1,0:T(8,128)(2,1)}, u32[]{:S(2)}) copy-start(bf16[2048,128]{1,0:T(8,128)(2,1)} %get-tuple-element.30) | copy-start | bytes 1572868
  98.2 3.6 %copy-start.4 = (bf16[2048,128]{1,0:T(8,128)(2,1)S(1)}, bf16[2048,128]{1,0:T(8,128)(2,1)}, u32[]{:S(2)}) copy-start(bf16[2048,128]{1,0:T(8,128)(2,1)} %get-tuple-element.32) | copy-start | bytes 1572868
  98.2 3.6 %copy-start.5 = (bf16[2048,128]{1,0:T(8,128)(2,1)S(1)}, bf16[2048,128]{1,0:T(8,128)(2,1)}, u32[]{:S(2)}) copy-start(bf16[2048,128]{1,0:T(8,128)(2,1)} %get-tuple-element.34) | copy-start | bytes 1572868
  101.8 3.3 %copy-start.7 = (bf16[576,2048]{1,0:T(8,128)(2,1)S(1)}, bf16[576,2048]{1,0:T(8,128)(2,1)}, u32[]{:S(2)}) copy-start(bf16[576,2048]{1,0:T(8,128)(2,1)} %convolution_convert_fusion.3) | copy-start | bytes 7077892
  109.6 58.4 %all-to-all-start.1 = ((bf16[4,144,2048]{2,1,0:T(8,128)(2,1)}), bf16[4,144,2048]{2,1,0:T(8,128)(2,1)}, u32[]{:S(2)}, u32[]{:S(2)}) async-start(bf16[4,144,2048]{2,1,0:T(8,128)(2,1)} %bitcast.59), calls=%async_computation.1 | async-start | bytes 4718592 | tf_op jit(solution)/shard_map/all_to_all | solution.py:200
  117.1 25.4 %collective-permute-start.1 = (bf16[256,2048]{1,0:T(8,128)(2,1)S(1)}, bf16[256,2048]{1,0:T(8,128)(2,1)S(1)}, u32[]{:S(2)}, u32[]{:S(2)}) collective-permute-start(bf16[256,2048]{1,0:T(8,128)(2,1)S(1)} %get-tuple-element.24), channel_id=1, source_target_pairs={{0,3},{1,2},{2,1},{3,0},{4,7},{5,6},{6,5},{7,4},{8,11},{9,10},{10,... | collective-permute-start | bytes 3145736 | tf_op jit(solution)/shard_map/ppermute | solution.py:111
  118.3 46.9 %collective-permute-start.2 = (bf16[256,2048]{1,0:T(8,128)(2,1)S(1)}, bf16[256,2048]{1,0:T(8,128)(2,1)S(1)}, u32[]{:S(2)}, u32[]{:S(2)}) collective-permute-start(bf16[256,2048]{1,0:T(8,128)(2,1)S(1)} %get-tuple-element.26), channel_id=1, source_target_pairs={{0,2},{1,3},{2,0},{3,1},{4,6},{5,7},{6,4},{7,5},{8,10},{9,11},{10,... | collective-permute-start | bytes 3145736 | tf_op jit(solution)/shard_map/ppermute | solution.py:111
  118.8 46.3 %collective-permute-start.3 = (bf16[256,2048]{1,0:T(8,128)(2,1)S(1)}, bf16[256,2048]{1,0:T(8,128)(2,1)S(1)}, u32[]{:S(2)}, u32[]{:S(2)}) collective-permute-start(bf16[256,2048]{1,0:T(8,128)(2,1)S(1)} %get-tuple-element.25), channel_id=1, source_target_pairs={{0,1},{1,0},{2,3},{3,2},{4,5},{5,4},{6,7},{7,6},{8,9},{9,8},{10,11... | collective-permute-start | bytes 3145736 | tf_op jit(solution)/shard_map/ppermute | solution.py:111
where the time goes:
time: 176 us; the launch traced here: 172 us
  waiting for transfers between devices  64.4 us (37%)
  matrix products  34.9 us (20%)
  starting transfers between devices  20.7 us (12%)
  blocking collectives  19.7 us (11%)
  other arithmetic  16.9 us (10%)
  local copies, waits for them, and re-layouts  14.9 us (8%)
    ppermute x11, waiting for transfers between devices, swapped(): return lax.ppermute(x, axis, [(i, i ^ mask) for i in range(peers)])  64.4 us
    psum x1, blocking collectives, conv_half(): lax.psum((jnp.sum(filtered, axis=1), jnp.sum(filtered * filtered, axis=1)...  19.7 us
    dot_general x2, matrix products, one_expert(): jnp.dot(inner, down, preferred_element_type=jnp.float32)  11.3 us
    dot_general x2, matrix products, one_expert(): gate_act = jnp.dot(rows, gate, preferred_element_type=jnp.float32)  8.26 us
    ppermute x11, starting transfers between devices, swapped(): return lax.ppermute(x, axis, [(i, i ^ mask) for i in range(peers)])  6.94 us
    slice x4, local copies, waits for them, and re-layouts, partner_weights(): gate = jnp.concatenate([piece[:, :share] for piece in gate_ups], 1)  5.62 us
    all_to_all x1, starting transfers between devices, pair_half(): lax.all_to_all(combined.astype(jnp.bfloat16).reshape(groups, capacity, mo...  5.24 us
    all_to_all x1, starting transfers between devices, pair_half(): lax.all_to_all(sent.reshape(groups, capacity, -1), 'ep', split_axis=0, co...  4.95 us
  transfers between devices with their start and end apart: 14, of which 4 were waited for; matrix products, arithmetic and copies ran while one was open for 31% of the time, Pallas kernels for 0%

commit v1 on v0

v1 whole, which is shorter than its diff:
```python
import functools

import jax
import jax.numpy as jnp
from jax import lax
from jax.experimental import pallas as pl
from jax.experimental.pallas import tpu as pltpu
from jax.sharding import PartitionSpec as P

GROUPS = 4
TOP = 2
LANES = 128
HALO = 32
MESH = pl.DeviceIdType.MESH
F32 = jnp.float32
BF16 = jnp.bfloat16


def passed_along(x, axis, by):
    peers = lax.axis_size(axis)
    pairs = [(i, i + by) for i in range(peers) if 0 <= i + by < peers]
    return lax.ppermute(x, axis, pairs)


def gated_rows(value, gate):
    return (value.astype(jnp.float32) * jax.nn.sigmoid(gate.astype(jnp.float32))).astype(
        jnp.bfloat16
    )


def conv_half(conv_value, conv_gate, earlier, depth_weight, norm_gain, norm_shift, conv_out_weight):
    channels = conv_value.shape[1]
    length = conv_value.shape[0]
    first_col = lax.axis_index("tp") * channels
    taps = lax.dynamic_slice_in_dim(depth_weight, first_col, channels, 1)
    gains = lax.dynamic_slice_in_dim(norm_gain, first_col, channels, 0)
    shifts = lax.dynamic_slice_in_dim(norm_shift, first_col, channels, 0)
    reach = taps.shape[0] - 1
    gated = gated_rows(conv_value, conv_gate)
    padded = jnp.concatenate([earlier, gated], 0).astype(jnp.float32)
    filtered = taps[0] * padded[0:length]
    for offset in range(1, reach + 1):
        filtered = filtered + taps[offset] * padded[offset : offset + length]
    sums, squares = lax.psum(
        (jnp.sum(filtered, axis=1), jnp.sum(filtered * filtered, axis=1)), "tp"
    )
    all_channels = channels * lax.axis_size("tp")
    center = (sums / all_channels)[:, None]
    spread = (squares / all_channels)[:, None] - center * center
    normed = (filtered - center) * lax.rsqrt(spread + 1e-05) * gains + shifts
    activated = jax.nn.silu(normed).astype(jnp.bfloat16)
    partial_value = jnp.dot(activated, conv_out_weight, preferred_element_type=jnp.float32)
    return partial_value.astype(jnp.bfloat16)


def swapped(x, axis, mask):
    peers = lax.axis_size(axis)
    return lax.ppermute(x, axis, [(i, i ^ mask) for i in range(peers)])


def scattered_sum(partial):
    peers = lax.axis_size("tp")
    me = lax.axis_index("tp")
    size = partial.shape[0] // peers
    total = lax.dynamic_slice_in_dim(partial, me * size, size, 0).astype(jnp.float32)
    for mask in range(peers - 1, 0, -1):
        block = lax.dynamic_slice_in_dim(partial, (me ^ mask) * size, size, 0)
        total = total + swapped(block, "tp", mask).astype(jnp.float32)
    return total.astype(jnp.bfloat16)


def moe_half(moe_input, moe_gain, route_experts, route_scores, expert_gate, expert_up, expert_down):
    rows = moe_input.shape[0]
    model_width = moe_input.shape[1]
    experts_all = lax.axis_size("ep")
    capacity = 2 * (3 * TOP * rows // (4 * experts_all))
    widened = moe_input.astype(jnp.float32)
    normal_in = (
        widened * lax.rsqrt(jnp.mean(widened * widened, axis=-1, keepdims=True) + 1e-06) * moe_gain
    ).astype(jnp.bfloat16)
    chosen = route_experts.reshape(-1)
    onehot = (chosen[:, None] == jnp.arange(experts_all, dtype=jnp.int32)[None, :]).astype(
        jnp.int32
    )
    slot_rank = jnp.sum(jnp.cumsum(onehot, axis=0) * onehot, axis=-1) - 1
    slot_index = jnp.where(
        slot_rank < capacity, chosen * capacity + slot_rank, experts_all * capacity
    )
    source_row = jnp.arange(rows * TOP, dtype=jnp.int32) // TOP
    slot_token = (
        jnp.full((experts_all * capacity,), rows, jnp.int32)
        .at[slot_index]
        .set(source_row, mode="drop")
    )
    padded_in = jnp.concatenate([normal_in, jnp.zeros((1, model_width), jnp.bfloat16)], 0)
    send_buffer = padded_in[slot_token].reshape(experts_all, capacity, model_width)
    arrived = lax.all_to_all(send_buffer, "ep", split_axis=0, concat_axis=0, tiled=True)
    flat_rows = arrived.reshape(-1, model_width)
    gate_act = jnp.dot(flat_rows, expert_gate[0], preferred_element_type=jnp.float32)
    up_act = jnp.dot(flat_rows, expert_up[0], preferred_element_type=jnp.float32)
    inner = (jax.nn.silu(gate_act) * up_act).astype(jnp.bfloat16)
    result = jnp.dot(inner, expert_down[0], preferred_element_type=jnp.float32).astype(jnp.bfloat16)
    returned = lax.all_to_all(
        result.reshape(arrived.shape), "ep", split_axis=0, concat_axis=0, tiled=True
    )
    returned_flat = jnp.concatenate(
        [
            returned.reshape(experts_all * capacity, model_width),
            jnp.zeros((1, model_width), jnp.bfloat16),
        ],
        0,
    )
    picked = returned_flat[slot_index].reshape(rows, TOP, model_width)
    group_gate = jax.nn.sigmoid(route_scores[:, 0])
    first_weight = (group_gate * jax.nn.sigmoid(route_scores[:, 1]))[:, None]
    second_weight = (group_gate * jax.nn.sigmoid(-route_scores[:, 1]))[:, None]
    combined = first_weight * picked[:, 0].astype(jnp.float32) + second_weight * picked[
        :, 1
    ].astype(jnp.float32)
    return combined.astype(jnp.bfloat16)


def sigmoid(v):
    return 1.0 / (1.0 + jnp.exp(-v))


def fused(
    cap,
    value_hbm,
    gate_hbm,
    taps_ref,
    gain_ref,
    shift_ref,
    wout_hbm,
    moe_hbm,
    mgain_ref,
    experts_ref,
    scores_ref,
    egate_hbm,
    eup_hbm,
    edown_hbm,
    conv_ref,
    moe_ref,
    value,
    gate,
    gpad,
    gin,
    halo,
    wide,
    filt,
    act,
    wout,
    tokens,
    normal,
    slots,
    wpieces,
    send,
    recv,
    wsend,
    wrecv,
    ogate,
    oup,
    odown,
    pgu,
    pdown,
    inner,
    result,
    ret,
    local_sem,
    zs,
    zr,
    us,
    ur,
    rs,
    rr,
    xs,
    xr,
    ys,
    yr,
    ds,
    dr,
    es,
    er,
    gs,
    gr,
    hs,
    hr,
    cs,
    cr,
):
    ep = lax.axis_index("ep")
    tp = lax.axis_index("tp")
    last_ep = lax.axis_size("ep") - 1
    z = ep // TOP
    x = lax.rem(ep, TOP)
    core = lax.rem(tp, 2)
    y = tp // 2
    core_peer = y * 2 + (1 - core)
    y_peer = (1 - y) * 2 + core
    diag = (1 - y) * 2 + (1 - core)
    lo = z < 2
    rows, width = tokens.shape
    length, chans = value.shape
    tile = gin.shape[0] - HALO
    share = pgu.shape[1] // 8
    wpad = wsend.shape[2]

    def at(e, t):
        return {"ep": e, "tp": t}

    def remote(src, dst, ssem, rsem, e, t):
        return pltpu.make_async_remote_copy(
            src_ref=src, dst_ref=dst, send_sem=ssem, recv_sem=rsem,
            device_id=at(e, t), device_id_type=MESH,
        )

    loads = [
        pltpu.make_async_copy(moe_hbm, tokens, local_sem.at[0]),
        pltpu.make_async_copy(value_hbm, value, local_sem.at[1]),
        pltpu.make_async_copy(gate_hbm, gate, local_sem.at[2]),
        pltpu.make_async_copy(egate_hbm, ogate, local_sem.at[3]),
        pltpu.make_async_copy(eup_hbm, oup, local_sem.at[4]),
        pltpu.make_async_copy(edown_hbm, odown, local_sem.at[5]),
        pltpu.make_async_copy(wout_hbm, wout.at[tp], local_sem.at[6]),
    ]
    for load in loads:
        load.start()

    barrier = pltpu.get_barrier_semaphore()

    def greet(e, t):
        pl.semaphore_signal(barrier, inc=1, device_id=at(e, t), device_id_type=MESH)

    for step in range(1, GROUPS):
        greet(lax.rem(z + step, GROUPS) * TOP + x, tp)
    greet(z * TOP + 1 - x, tp)
    greet(ep, core_peer)
    greet(ep, y_peer)
    greet(ep, diag)

    @pl.when(ep < last_ep)
    def _():
        greet(ep + 1, 0)

    first_tp = jnp.logical_and(ep > 0, tp == 0)

    @pl.when(first_tp)
    def _():
        for t in range(4):
            greet(ep - 1, t)

    expected = (
        GROUPS + 3
        + jnp.where(ep < last_ep, 1, 0)
        + jnp.where(first_tp, 4, 0)
    )
    pl.semaphore_wait(barrier, expected)

    depth = width // 2
    half = share // 2

    def piece(j, q, gates, ups, downs, wide_cols):
        c = j % 2
        kind = j // 2
        if kind == 2:
            return downs.at[pl.ds(pl.multiple_of(q * share + c * half, half), half), :]
        span = pl.ds(c * depth, depth)
        ref = gates if kind == 0 else ups
        if wide_cols:
            col = pl.multiple_of(q * (2 * share) + kind * share, share)
        else:
            col = pl.multiple_of(q * share, share)
        return ref.at[span, pl.ds(col, share)]

    def held(j, q):
        return piece(j, q, pgu, pgu, pdown, True)

    pieces = 6
    hop_x = [
        remote(
            piece(j, tp, egate_hbm, eup_hbm, edown_hbm, False),
            held(j, tp), xs.at[j], xr.at[j], z * TOP + 1 - x, tp,
        )
        for j in range(pieces)
    ]
    hop_y = [remote(held(j, tp), held(j, tp), ys.at[j], yr.at[j], ep, y_peer) for j in range(pieces)]
    hop_d = [remote(held(j, tp), held(j, tp), ds.at[j], dr.at[j], ep, core_peer) for j in range(pieces)]
    hop_e = [
        remote(held(j, y_peer), held(j, y_peer), es.at[j], er.at[j], ep, core_peer)
        for j in range(pieces)
    ]
    for hop in hop_x:
        hop.start()

    first = jnp.broadcast_to(experts_ref[0:1, :], (8, rows))
    group_id = lax.broadcasted_iota(jnp.int32, (8, rows), 0)
    member = jnp.logical_and(first >= group_id * TOP, first < (group_id + 1) * TOP)
    before = (
        lax.broadcasted_iota(jnp.int32, (rows, rows), 0)
        < lax.broadcasted_iota(jnp.int32, (rows, rows), 1)
    ).astype(F32).astype(BF16)
    rank = jnp.dot(member.astype(F32).astype(BF16), before, preferred_element_type=F32)
    keep = jnp.logical_and(member, rank < cap)
    slots[...] = jnp.where(keep, rank, -1.0)
    group_gate = sigmoid(scores_ref[0:1, :])
    first_weight = group_gate * sigmoid(scores_ref[1:2, :])
    second_weight = group_gate * sigmoid(-scores_ref[1:2, :])
    in_order = experts_ref[0:1, :] < experts_ref[1:2, :]
    low = jnp.where(in_order, first_weight, second_weight)
    high = jnp.where(in_order, second_weight, first_weight)
    parts = []
    for weight in (low, high):
        for _ in range(3):
            rounded = weight.astype(BF16).astype(F32)
            parts.append(rounded)
            weight = weight - rounded
    nothing = jnp.zeros((2, rows), F32)
    wpieces[...] = jnp.concatenate(parts + [nothing], 0).astype(BF16)

    loads[0].wait()
    strip = 32

    def norm_rows(i, carry):
        span = pl.ds(pl.multiple_of(i * strip, strip), strip)
        wide_rows = tokens[span, :].astype(F32)
        scale = lax.rsqrt(
            jnp.sum(wide_rows * wide_rows, axis=1, keepdims=True) * (1.0 / width) + 1e-06
        )
        normal[span, :] = (wide_rows * scale * mgain_ref[...]).astype(BF16)
        return carry

    lax.fori_loop(0, rows // strip, norm_rows, 0)

    zx = z + 1 - 2 * lax.rem(z, 2)
    block = 512

    def dispatch(k, carry):
        d = jnp.where(
            k == 0, jnp.where(lo, 3, 0),
            jnp.where(k == 1, zx, jnp.where(k == 2, jnp.where(lo, 2, 1), z)),
        )
        slot = slots[pl.ds(d, 1), :]
        pick = (
            lax.broadcasted_iota(jnp.int32, (wpad, rows), 0).astype(F32)
            == jnp.broadcast_to(slot, (wpad, rows))
        ).astype(F32).astype(BF16)
        weights = lax.dot_general(
            wpieces[...], pick, (((1,), (1,)), ((), ())), preferred_element_type=F32
        )
        for n in range(width // block):
            cols = pl.ds(n * block, block)
            chosen = jnp.dot(pick[:cap], normal[:, cols], preferred_element_type=F32)
            send[d, :, cols] = chosen.astype(BF16)
        wsend[d] = weights

        @pl.when(k < 3)
        def _():
            remote(
                send.at[d], recv.at[z], zs.at[d], zr.at[z], d * TOP + x, tp
            ).start()
            remote(
                wsend.at[d], wrecv.at[z], us.at[d], ur.at[z], d * TOP + x, tp
            ).start()

        return carry

    lax.fori_loop(0, 4, dispatch, 0)
    recv[z] = send[z]
    wrecv[z] = wsend[z]

    loads[1].wait()
    loads[2].wait()
    gpad[0:HALO, :] = jnp.zeros((HALO, chans), BF16)
    gstrip = 64

    def gate_rows(i, carry):
        span = pl.ds(pl.multiple_of(i * gstrip, gstrip), gstrip)
        out = pl.ds(pl.multiple_of(i * gstrip + HALO, HALO), gstrip)
        gpad[out, :] = (value[span, :].astype(F32) * sigmoid(gate[span, :].astype(F32))).astype(BF16)
        return carry

    lax.fori_loop(0, length // gstrip, gate_rows, 0)
    my_cols = pl.ds(pl.multiple_of(tp * chans, LANES), chans)

    def window(t):
        return pl.ds(pl.multiple_of(t * tile, HALO), tile + HALO)

    gated_copies = [
        remote(gpad.at[window(t)], gin.at[:, my_cols], gs.at[i], gr.at[i], ep, t)
        for i, t in enumerate((core_peer, y_peer, diag))
    ]
    for copy in gated_copies:
        copy.start()

    def halo_copy(t, e, c):
        cols = pl.ds(pl.multiple_of(c * chans, LANES), chans)
        return remote(
            gpad.at[pl.ds(length, HALO)], halo.at[:, cols], hs, hr.at[c], e, t
        )

    @pl.when(ep < last_ep)
    def _():
        halo_copy(0, ep + 1, tp).start()

    gin[:, my_cols] = gpad[window(tp), :]

    for g in range(GROUPS):
        ret[g, cap:, :] = jnp.zeros((ret.shape[1] - cap, width), BF16)

    own_wout = wout.at[tp]
    out_y = remote(own_wout, own_wout, cs.at[0], cr.at[0], ep, y_peer)
    out_d = remote(own_wout, own_wout, cs.at[1], cr.at[1], ep, core_peer)
    out_e = remote(wout.at[y_peer], wout.at[y_peer], cs.at[2], cr.at[2], ep, core_peer)

    taps_count = taps_ref.shape[0]
    lane_blocks = gin.shape[1] // LANES
    frows = 64

    def widen():
        for copy in gated_copies:
            copy.wait_recv()

        @pl.when(first_tp)
        def _():
            for c in range(4):
                halo_copy(0, ep, c).wait_recv()
            gin[0:HALO, :] = halo[...]

        for b in range(lane_blocks):
            wide[b] = gin[:, b * LANES : (b + 1) * LANES].astype(F32)

    def filter_block(b, carry):
        for r in range(tile // frows):
            total = jnp.zeros((frows, LANES), F32)
            for k in range(taps_count):
                start = r * frows + HALO - taps_count + 1 + k
                tap = taps_ref[pl.ds(k, 1), pl.ds(pl.multiple_of(b * LANES, LANES), LANES)]
                total = total + tap * wide[b, pl.ds(start, frows), :]
            filt[b, pl.ds(r * frows, frows), :] = total
        return carry

    def activate(i, carry):
        span = pl.ds(pl.multiple_of(i * strip, strip), strip)
        total = filt[0, span, :]
        squares = total * total
        for b in range(1, lane_blocks):
            part = filt[b, span, :]
            total = total + part
            squares = squares + part * part
        count = 1.0 / (lane_blocks * LANES)
        center = jnp.sum(total, axis=1, keepdims=True) * count
        spread = jnp.sum(squares, axis=1, keepdims=True) * count - center * center
        scale = lax.rsqrt(spread + 1e-05)
        for b in range(lane_blocks):
            cols = slice(b * LANES, (b + 1) * LANES)
            normed = (filt[b, span, :] - center) * scale * gain_ref[:, cols] + shift_ref[:, cols]
            act[span, cols] = (normed * sigmoid(normed)).astype(BF16)
        return carry

    for j in range(pieces):
        hop_x[j].wait_recv()
        hop_y[j].start()
        hop_d[j].start()
        if j > 0:
            hop_y[j - 1].wait_recv()
            hop_e[j - 1].start()
        if j == 1:
            widen()
            lax.fori_loop(0, 2, filter_block, 0)
        if 2 <= j < 5:
            lax.fori_loop(2 * j - 2, 2 * j, filter_block, 0)
        if j == 5:
            lax.fori_loop(0, tile // strip, activate, 0)
    loads[6].wait()
    out_y.start()
    out_d.start()
    hop_y[pieces - 1].wait_recv()
    hop_e[pieces - 1].start()
    for load in loads[3:6]:
        load.wait()
    for j in range(pieces):
        hop_d[j].wait_recv()
        hop_e[j].wait_recv()

    ff = ogate.shape[1]
    even = x == 0
    nb = 256

    def expert(i, carry):
        even_z = lax.rem(z, 2) == 0
        s = jnp.where(
            i == 0, jnp.where(even_z, 3, 0),
            jnp.where(
                i == 1, lax.rem(z + 2, GROUPS),
                jnp.where(i == 2, jnp.where(even_z, 1, 2), z),
            ),
        )

        @pl.when(i < 3)
        def _():
            remote(send.at[s], recv.at[s], zs.at[s], zr.at[s], s * TOP + x, tp).wait_recv()
            remote(wsend.at[s], wrecv.at[s], us.at[s], ur.at[s], s * TOP + x, tp).wait_recv()

        w8 = wrecv[s]
        w_low = w8[0:1] + w8[1:2] + w8[2:3]
        w_high = w8[3:4] + w8[4:5] + w8[5:6]
        mine = jnp.where(even, w_low, w_high)
        theirs = jnp.where(even, w_high, w_low)
        mine = jnp.transpose(jnp.broadcast_to(mine, (LANES, wpad)))[:cap]
        theirs = jnp.transpose(jnp.broadcast_to(theirs, (LANES, wpad)))[:cap]
        mine2 = jnp.concatenate([mine] * (nb // LANES), 1)
        theirs1 = jnp.concatenate([theirs] * (share // LANES), 1)
        here = recv[s]
        for n in range(ff // nb):
            cols = pl.ds(n * nb, nb)
            g = jnp.dot(here, ogate[:, cols], preferred_element_type=F32)
            u = jnp.dot(here, oup[:, cols], preferred_element_type=F32)
            inner[:, cols] = (g * sigmoid(g) * u * mine2).astype(BF16)
        for q in range(4):
            gu = jnp.dot(
                here, pgu[:, pl.ds(q * 2 * share, 2 * share)], preferred_element_type=F32
            )
            g = gu[:, :share]
            u = gu[:, share:]
            inner[:, pl.ds(ff + q * share, share)] = (g * sigmoid(g) * u * theirs1).astype(BF16)
        for n in range(width // nb):
            cols = pl.ds(n * nb, nb)
            total = jnp.dot(inner[:, :ff], odown[:, cols], preferred_element_type=F32) + jnp.dot(
                inner[:, ff:], pdown[:, cols], preferred_element_type=F32
            )
            result[s, :, cols] = total.astype(BF16)

        @pl.when(i < 3)
        def _():
            remote(
                result.at[s], ret.at[z, pl.ds(0, cap)], rs.at[s], rr.at[z], s * TOP + x, tp
            ).start()

        return carry

    lax.fori_loop(0, 4, expert, 0)
    ret[z, pl.ds(0, cap), :] = result[z]

    out_y.wait_recv()
    out_e.start()
    out_d.wait_recv()
    out_e.wait_recv()

    def project(n, carry):
        cols = pl.ds(pl.multiple_of(n * nb, nb), nb)
        total = jnp.dot(act[:, 0:chans], wout[0, :, cols], preferred_element_type=F32)
        for t in range(1, 4):
            total = total + jnp.dot(
                act[:, t * chans : (t + 1) * chans], wout[t, :, cols], preferred_element_type=F32
            )
        conv_ref[:, cols] = total.astype(BF16)
        return carry

    lax.fori_loop(0, width // nb, project, 0)

    def put(g):
        slot = jnp.transpose(jnp.broadcast_to(slots[pl.ds(g, 1), :], (LANES, rows)))
        lane = lax.broadcasted_iota(jnp.int32, (rows, LANES), 1).astype(F32)
        return jnp.concatenate(
            [(slot == lane + float(b * LANES)).astype(F32).astype(BF16) for b in range(wpad // LANES)],
            1,
        )

    def returned(g):
        return remote(
            result.at[g], ret.at[g, pl.ds(0, cap)], rs.at[g], rr.at[g], g * TOP + x, tp
        )

    third = jnp.where(lo, 3, 0)
    last = jnp.where(lo, 2, 1)

    def add_back(g, fresh):
        chosen = put(g)
        for n in range(width // nb):
            cols = pl.ds(n * nb, nb)
            rows_back = jnp.dot(chosen, ret[g, :, cols], preferred_element_type=F32)
            if fresh:
                moe_ref[:, cols] = rows_back.astype(BF16)
            else:
                moe_ref[:, cols] = (moe_ref[:, cols].astype(F32) + rows_back).astype(BF16)

    add_back(z, True)

    def rest(i, carry):
        g = jnp.where(i == 0, zx, jnp.where(i == 1, third, last))
        returned(g).wait_recv()
        add_back(g, False)
        return carry

    lax.fori_loop(0, 3, rest, 0)

    for step in range(1, GROUPS):
        s = lax.rem(z + step, GROUPS)
        remote(send.at[s], recv.at[s], zs.at[s], zr.at[s], s * TOP + x, tp).wait_send()
        remote(wsend.at[s], wrecv.at[s], us.at[s], ur.at[s], s * TOP + x, tp).wait_send()
        returned(s).wait_send()
    for j in range(pieces):
        hop_x[j].wait_send()
        hop_y[j].wait_send()
        hop_d[j].wait_send()
        hop_e[j].wait_send()
    for copy in gated_copies:
        copy.wait_send()

    @pl.when(ep < last_ep)
    def _():
        halo_copy(0, ep + 1, tp).wait_send()

    out_y.wait_send()
    out_d.wait_send()
    out_e.wait_send()


def one_kernel(
    conv_value, conv_gate, depth_weight, norm_gain, norm_shift, conv_out_weight,
    moe_input, moe_gain, route_experts, route_scores, expert_gate, expert_up, expert_down,
):
    length, chans = conv_value.shape
    peers = lax.axis_size("tp")
    tile = length // peers
    all_chans = chans * peers
    rows, width = moe_input.shape
    ff = expert_gate.shape[2]
    cap = 2 * (3 * TOP * rows // (4 * lax.axis_size("ep")))
    wpad = -(-cap // LANES) * LANES
    vmem = pl.BlockSpec(memory_space=pltpu.VMEM)
    hbm = pl.BlockSpec(memory_space=pl.ANY)
    dma = pltpu.SemaphoreType.DMA
    blocks = all_chans // LANES
    return pl.pallas_call(
        functools.partial(fused, cap),
        out_shape=(
            jax.ShapeDtypeStruct((tile, width), BF16),
            jax.ShapeDtypeStruct((rows, width), BF16),
        ),
        in_specs=[hbm, hbm, vmem, vmem, vmem, hbm, hbm, vmem, vmem, vmem, hbm, hbm, hbm],
        out_specs=(vmem, vmem),
        scratch_shapes=[
            pltpu.VMEM((length, chans), BF16),
            pltpu.VMEM((length, chans), BF16),
            pltpu.VMEM((length + HALO, chans), BF16),
            pltpu.VMEM((tile + HALO, all_chans), BF16),
            pltpu.VMEM((HALO, all_chans), BF16),
            pltpu.VMEM((blocks, tile + HALO, LANES), F32),
            pltpu.VMEM((blocks, tile, LANES), F32),
            pltpu.VMEM((tile, all_chans), BF16),
            pltpu.VMEM((peers, chans, width), BF16),
            pltpu.VMEM((rows, width), BF16),
            pltpu.VMEM((rows, width), BF16),
            pltpu.VMEM((8, rows), F32),
            pltpu.VMEM((8, rows), BF16),
            pltpu.VMEM((GROUPS, cap, width), BF16),
            pltpu.VMEM((GROUPS, cap, width), BF16),
            pltpu.VMEM((GROUPS, 8, wpad), F32),
            pltpu.VMEM((GROUPS, 8, wpad), F32),
            pltpu.VMEM((width, ff), BF16),
            pltpu.VMEM((width, ff), BF16),
            pltpu.VMEM((ff, width), BF16),
            pltpu.VMEM((width, 2 * ff), BF16),
            pltpu.VMEM((ff, width), BF16),
            pltpu.VMEM((cap, 2 * ff), BF16),
            pltpu.VMEM((GROUPS, cap, width), BF16),
            pltpu.VMEM((GROUPS, wpad, width), BF16),
            dma((7,)),
            dma((GROUPS,)), dma((GROUPS,)),
            dma((GROUPS,)), dma((GROUPS,)),
            dma((GROUPS,)), dma((GROUPS,)),
            dma((6,)), dma((6,)),
            dma((6,)), dma((6,)),
            dma((6,)), dma((6,)),
            dma((6,)), dma((6,)),
            dma((3,)), dma((3,)),
            dma(()), dma((4,)),
            dma((3,)), dma((3,)),
        ],
        compiler_params=pltpu.CompilerParams(
            collective_id=0, has_side_effects=True, vmem_limit_bytes=63 * 1024 * 1024
        ),
        name="fused",
    )(
        conv_value, conv_gate, depth_weight, norm_gain[None, :], norm_shift[None, :],
        conv_out_weight, moe_input, moe_gain[None, :], route_experts.T, route_scores.T,
        expert_gate[0], expert_up[0], expert_down[0],
    )


def on_device(
    conv_value,
    conv_gate,
    depth_weight,
    norm_gain,
    norm_shift,
    conv_out_weight,
    moe_input,
    moe_gain,
    route_experts,
    route_scores,
    expert_gate,
    expert_up,
    expert_down,
):
    conv_args = (conv_value, conv_gate, depth_weight, norm_gain, norm_shift, conv_out_weight)
    moe_args = (
        moe_input, moe_gain, route_experts, route_scores, expert_gate, expert_up, expert_down
    )
    if lax.axis_size("ep") == GROUPS * TOP and lax.axis_size("tp") == 4:
        return one_kernel(*conv_args, *moe_args)
    last = conv_value.shape[0] - depth_weight.shape[0] + 1
    earlier = passed_along(gated_rows(conv_value[last:], conv_gate[last:]), "ep", 1)
    partial = conv_half(conv_value, conv_gate, earlier, *conv_args[2:])
    return (scattered_sum(partial), moe_half(*moe_args))


def solution(mesh):
    in_specs = (
        P("ep", "tp"),
        P("ep", "tp"),
        P(),
        P(),
        P(),
        P("tp", None),
        P(("ep", "tp"), None),
        P(),
        P(("ep", "tp"), None),
        P(("ep", "tp"), None),
        P("ep", None, None),
        P("ep", None, None),
        P("ep", None, None),
    )
    out_specs = (P(("ep", "tp"), None), P(("ep", "tp"), None))
    return jax.shard_map(
        on_device, mesh=mesh, in_specs=in_specs, out_specs=out_specs, check_vma=False
    )
```

time: 176 us -> 131 us (0.74); the launches traced: 172 us -> 131 us
  Pallas kernels: 0 us -> 127 us
  waiting for transfers between devices: 64.4 us -> 0 us
  matrix products: 34.9 us -> 0 us
  starting transfers between devices: 20.7 us -> 0 us
  blocking collectives: 19.7 us -> 0 us
  other arithmetic: 16.9 us -> 0 us
  local copies, waits for them, and re-layouts: 14.9 us -> 3.57 us
    pallas_call x0 -> x1, Pallas kernels: none -> 127 us  [one_kernel(): pl.pallas_call(functools.partial(fused, cap), out_shape=(jax.ShapeDtypeSt...]
    ppermute x12 -> x0, waiting for transfers between devices: 64.4 us -> none  [the longest x11 64.4 us: swapped(): return lax.ppermute(x, axis, [(i, i ^ mask) for i in range(peers)])]
    dot_general x9 -> x0, matrix products: 34.9 us -> none  [the longest x2 11.3 us: one_expert(): jnp.dot(inner, down, preferred_element_type=jnp.float32)]
    psum x1 -> x0, blocking collectives: 19.7 us -> none  [conv_half(): lax.psum((jnp.sum(filtered, axis=1), jnp.sum(filtered * filtered, axis=1)...]
    ppermute x12 -> x0, starting transfers between devices: 10.5 us -> none  [the longest x11 6.94 us: swapped(): return lax.ppermute(x, axis, [(i, i ^ mask) for i in range(peers)])]
    all_to_all x2 -> x0, starting transfers between devices: 10.2 us -> none  [the longest x1 5.24 us: pair_half(): lax.all_to_all(combined.astype(jnp.bfloat16).reshape(groups, capacity, mo...]
    slice x6 -> x0, local copies, waits for them, and re-layouts: 8.01 us -> none  [the longest x4 5.62 us: partner_weights(): gate = jnp.concatenate([piece[:, :share] for piece in gate_ups], 1)]
    convert_element_type x8 -> x0, other arithmetic: 7.52 us -> none  [the longest x1 2.9 us: scattered_sum(): return total.astype(jnp.bfloat16)]
  transfers between devices with their start and end apart: 14 -> 0, of which waited for: 4 -> 0; matrix products, arithmetic and copies ran while one was open for 31% -> 0% of each run, Pallas kernels for 0% -> 0%
where the time goes in v1:
time: 131 us
  Pallas kernels  127 us (97%)
  local copies, waits for them, and re-layouts  3.57 us (3%)
    pallas_call x1, Pallas kernels, one_kernel(): pl.pallas_call(functools.partial(fused, cap), out_shape=(jax.ShapeDtypeSt...  127 us
    unnamed x4, local copies, waits for them, and re-layouts  3.57 us

profile of v1, /device:TPU:8, one launch (start us, length us, event | category | flops | bytes accessed | tf_op | source)
XLA Modules:
  0.0 131.0 jit_solution(661955991174609496)
XLA Ops:
  0.6 126.7 %fused.1 = (bf16[256,2048]{1,0:T(8,128)(2,1)}, bf16[384,2048]{1,0:T(8,128)(2,1)}) custom-call(bf16[1024,256]{1,0:T(8,128)(2,1)} %value_hbm.1, bf16[1024,256]{1,0:T(8,128)(2,1)} %gate_hbm.1, f32[31,1024]{1,0:T(8,128)} %taps_ref.1, f32[1,1024]{1,0:T(1,128)} %bitcast.12, f32[1,1024]{1,0:T(1,128)} %bitcast.13, bf16[256,2048]{1,0:T(8,128)(2,1)} %wout_hbm.1, ...), custom_call_target="tpu_custom_call" | custom-call | tf_op jit(solution)/shard_map/fused/pallas_call | solution.py:635
  127.4 0.0 copy-start
  127.4 2.4 %copy.17 = bf16[256,2048]{1,0:T(8,128)(2,1)} copy(bf16[256,2048]{1,0:T(8,128)(2,1)} %get-tuple-element.4) | data formatting | bytes 2097152
  129.8 0.0 copy-done
  129.8 1.1 copy.18
Async XLA Ops:
  127.4 2.4 %copy-start = (bf16[384,2048]{1,0:T(8,128)(2,1)S(1)}, bf16[384,2048]{1,0:T(8,128)(2,1)}, u32[]{:S(2)}) copy-start(bf16[384,2048]{1,0:T(8,128)(2,1)} %get-tuple-element.5) | copy-start | bytes 4718596

commit v2 on v1

--- a/solution.py
+++ b/solution.py
@@ -128,24 +128,31 @@
     cap,
     value_hbm,
     gate_hbm,
-    taps_ref,
-    gain_ref,
-    shift_ref,
+    taps_hbm,
+    gain_hbm,
+    shift_hbm,
     wout_hbm,
     moe_hbm,
-    mgain_ref,
-    experts_ref,
-    scores_ref,
+    mgain_hbm,
+    experts_hbm,
+    scores_hbm,
     egate_hbm,
     eup_hbm,
     edown_hbm,
     conv_ref,
     moe_ref,
+    taps_ref,
+    gain_ref,
+    shift_ref,
+    mgain_ref,
+    experts_ref,
+    scores_ref,
     value,
     gate,
     gpad,
     gin,
     halo,
+    edge,
     wide,
     filt,
     act,
@@ -214,6 +221,16 @@
             device_id=at(e, t), device_id_type=MESH,
         )
 
+    small = [
+        pltpu.make_async_copy(experts_hbm, experts_ref, local_sem.at[9]),
+        pltpu.make_async_copy(scores_hbm, scores_ref, local_sem.at[10]),
+        pltpu.make_async_copy(mgain_hbm, mgain_ref, local_sem.at[11]),
+        pltpu.make_async_copy(taps_hbm, taps_ref, local_sem.at[12]),
+        pltpu.make_async_copy(gain_hbm, gain_ref, local_sem.at[13]),
+        pltpu.make_async_copy(shift_hbm, shift_ref, local_sem.at[14]),
+    ]
+    for load in small[:3]:
+        load.start()
     loads = [
         pltpu.make_async_copy(moe_hbm, tokens, local_sem.at[0]),
         pltpu.make_async_copy(value_hbm, value, local_sem.at[1]),
@@ -222,8 +239,10 @@
         pltpu.make_async_copy(eup_hbm, oup, local_sem.at[4]),
         pltpu.make_async_copy(edown_hbm, odown, local_sem.at[5]),
         pltpu.make_async_copy(wout_hbm, wout.at[tp], local_sem.at[6]),
+        pltpu.make_async_copy(value_hbm.at[pl.ds(length - HALO, HALO)], edge.at[0], local_sem.at[7]),
+        pltpu.make_async_copy(gate_hbm.at[pl.ds(length - HALO, HALO)], edge.at[1], local_sem.at[8]),
     ]
-    for load in loads:
+    for load in loads[:1] + loads[7:] + loads[1:7] + small[3:]:
         load.start()
 
     barrier = pltpu.get_barrier_semaphore()
@@ -254,7 +273,6 @@
         + jnp.where(ep < last_ep, 1, 0)
         + jnp.where(first_tp, 4, 0)
     )
-    pl.semaphore_wait(barrier, expected)
 
     depth = width // 2
     half = share // 2
@@ -289,9 +307,10 @@
         remote(held(j, y_peer), held(j, y_peer), es.at[j], er.at[j], ep, core_peer)
         for j in range(pieces)
     ]
-    for hop in hop_x:
-        hop.start()
-
+
+    small[0].wait()
+    small[1].wait()
+    small[2].wait()
     first = jnp.broadcast_to(experts_ref[0:1, :], (8, rows))
     group_id = lax.broadcasted_iota(jnp.int32, (8, rows), 0)
     member = jnp.logical_and(first >= group_id * TOP, first < (group_id + 1) * TOP)
@@ -331,6 +350,21 @@
 
     lax.fori_loop(0, rows // strip, norm_rows, 0)
 
+    def halo_copy(t, e, c):
+        cols = pl.ds(pl.multiple_of(c * chans, LANES), chans)
+        return remote(edge.at[2], halo.at[:, cols], hs, hr.at[c], e, t)
+
+    loads[7].wait()
+    loads[8].wait()
+    edge[2] = (edge[0].astype(F32) * sigmoid(edge[1].astype(F32))).astype(BF16)
+    pl.semaphore_wait(barrier, expected)
+    for hop in hop_x:
+        hop.start()
+
+    @pl.when(ep < last_ep)
+    def _():
+        halo_copy(0, ep + 1, tp).start()
+
     zx = z + 1 - 2 * lax.rem(z, 2)
     block = 512
 
@@ -391,16 +425,6 @@
     ]
     for copy in gated_copies:
         copy.start()
-
-    def halo_copy(t, e, c):
-        cols = pl.ds(pl.multiple_of(c * chans, LANES), chans)
-        return remote(
-            gpad.at[pl.ds(length, HALO)], halo.at[:, cols], hs, hr.at[c], e, t
-        )
-
-    @pl.when(ep < last_ep)
-    def _():
-        halo_copy(0, ep + 1, tp).start()
 
     gin[:, my_cols] = gpad[window(tp), :]
 
@@ -465,6 +489,8 @@
             hop_y[j - 1].wait_recv()
             hop_e[j - 1].start()
         if j == 1:
+            for load in small[3:]:
+                load.wait()
             widen()
             lax.fori_loop(0, 2, filter_block, 0)
         if 2 <= j < 5:
@@ -629,7 +655,7 @@
     cap = 2 * (3 * TOP * rows // (4 * lax.axis_size("ep")))
     wpad = -(-cap // LANES) * LANES
     vmem = pl.BlockSpec(memory_space=pltpu.VMEM)
-    hbm = pl.BlockSpec(memory_space=pl.ANY)
+    hbm = pl.BlockSpec(memory_space=pltpu.HBM)
     dma = pltpu.SemaphoreType.DMA
     blocks = all_chans // LANES
     return pl.pallas_call(
@@ -638,14 +664,21 @@
             jax.ShapeDtypeStruct((tile, width), BF16),
             jax.ShapeDtypeStruct((rows, width), BF16),
         ),
-        in_specs=[hbm, hbm, vmem, vmem, vmem, hbm, hbm, vmem, vmem, vmem, hbm, hbm, hbm],
+        in_specs=[hbm] * 13,
         out_specs=(vmem, vmem),
         scratch_shapes=[
+            pltpu.VMEM(depth_weight.shape, F32),
+            pltpu.VMEM((1, all_chans), F32),
+            pltpu.VMEM((1, all_chans), F32),
+            pltpu.VMEM((1, width), F32),
+            pltpu.VMEM((TOP, rows), jnp.int32),
+            pltpu.VMEM((TOP, rows), F32),
             pltpu.VMEM((length, chans), BF16),
             pltpu.VMEM((length, chans), BF16),
             pltpu.VMEM((length + HALO, chans), BF16),
             pltpu.VMEM((tile + HALO, all_chans), BF16),
             pltpu.VMEM((HALO, all_chans), BF16),
+            pltpu.VMEM((3, HALO, chans), BF16),
             pltpu.VMEM((blocks, tile + HALO, LANES), F32),
             pltpu.VMEM((blocks, tile, LANES), F32),
             pltpu.VMEM((tile, all_chans), BF16),
@@ -666,7 +699,7 @@
             pltpu.VMEM((cap, 2 * ff), BF16),
             pltpu.VMEM((GROUPS, cap, width), BF16),
             pltpu.VMEM((GROUPS, wpad, width), BF16),
-            dma((7,)),
+            dma((15,)),
             dma((GROUPS,)), dma((GROUPS,)),
             dma((GROUPS,)), dma((GROUPS,)),
             dma((GROUPS,)), dma((GROUPS,)),
@@ -679,13 +712,18 @@
             dma((3,)), dma((3,)),
         ],
         compiler_params=pltpu.CompilerParams(
-            collective_id=0, has_side_effects=True, vmem_limit_bytes=63 * 1024 * 1024
+            collective_id=0, has_side_effects=True, vmem_limit_bytes=46 * 1024 * 1024
         ),
         name="fused",
     )(
-        conv_value, conv_gate, depth_weight, norm_gain[None, :], norm_shift[None, :],
-        conv_out_weight, moe_input, moe_gain[None, :], route_experts.T, route_scores.T,
-        expert_gate[0], expert_up[0], expert_down[0],
+        *(
+            pltpu.with_memory_space_constraint(a, pltpu.HBM)
+            for a in (
+                conv_value, conv_gate, depth_weight, norm_gain[None, :], norm_shift[None, :],
+                conv_out_weight, moe_input, moe_gain[None, :], route_experts.T, route_scores.T,
+                expert_gate[0], expert_up[0], expert_down[0],
+            )
+        )
     )
 
 

time: 131 us -> 126 us (0.962)
  the two profiles are of different devices: /device:TPU:8 before, /device:TPU:15 now
where the time goes in v2:
time: 126 us
  Pallas kernels  123 us (98%)
  local copies, waits for them, and re-layouts  2.11 us (2%)
    pallas_call x1, Pallas kernels, one_kernel(): pl.pallas_call(functools.partial(fused, cap), out_shape=(jax.ShapeDtypeSt...  123 us

profile of v2, /device:TPU:15, one launch (start us, length us, event | category | flops | bytes accessed | tf_op | source)
XLA Modules:
  0.0 126.0 jit_solution(150285582070637971)
XLA Ops:
  0.6 123.2 %fused.1 = (bf16[256,2048]{1,0:T(8,128)(2,1)S(1)}, bf16[384,2048]{1,0:T(8,128)(2,1)S(1)}) custom-call(bf16[1024,256]{1,0:T(8,128)(2,1)} %value_hbm.1, bf16[1024,256]{1,0:T(8,128)(2,1)} %gate_hbm.1, f32[31,1024]{1,0:T(8,128)} %taps_hbm.1, f32[1,1024]{1,0:T(1,128)} %bitcast.12, f32[1,1024]{1,0:T(1,128)} %bitcast.13, bf16[256,2048]{1,0:T(8,128)(2,1)} %wout_hbm.1, ...), custom_call_target="tpu_custom_call" | custom-call | tf_op jit(solution)/shard_map/fused/pallas_call | solution.py:661
  123.9 1.0 copy.17
  124.9 1.1 copy.18

commit v3 on v2

--- a/solution.py
+++ b/solution.py
@@ -12,6 +12,8 @@
 LANES = 128
 HALO = 32
 MESH = pl.DeviceIdType.MESH
+OUTWARD = ((1, 3), (2, 0), (3, 2))
+HOMEWARD = ((3, 3), (1, 0), (2, 2))
 F32 = jnp.float32
 BF16 = jnp.bfloat16
 
@@ -158,7 +160,7 @@
     act,
     wout,
     tokens,
-    normal,
+    raw,
     slots,
     wpieces,
     send,
@@ -205,7 +207,6 @@
     core_peer = y * 2 + (1 - core)
     y_peer = (1 - y) * 2 + core
     diag = (1 - y) * 2 + (1 - core)
-    lo = z < 2
     rows, width = tokens.shape
     length, chans = value.shape
     tile = gin.shape[0] - HALO
@@ -219,6 +220,28 @@
         return pltpu.make_async_remote_copy(
             src_ref=src, dst_ref=dst, send_sem=ssem, recv_sem=rsem,
             device_id=at(e, t), device_id_type=MESH,
+        )
+
+    def there(s):
+        return remote(send.at[s], recv.at[z], zs.at[s], zr.at[z], s * TOP + x, tp)
+
+    def here_from(s):
+        return remote(send.at[s], recv.at[s], zs.at[s], zr.at[s], s * TOP + x, tp)
+
+    def weights_there(s):
+        return remote(wsend.at[s], wrecv.at[z], us.at[s], ur.at[z], s * TOP + x, tp)
+
+    def weights_here(s):
+        return remote(wsend.at[s], wrecv.at[s], us.at[s], ur.at[s], s * TOP + x, tp)
+
+    def back(s):
+        return remote(
+            result.at[s], ret.at[z, pl.ds(0, cap)], rs.at[s], rr.at[z], s * TOP + x, tp
+        )
+
+    def returned(g):
+        return remote(
+            result.at[g], ret.at[g, pl.ds(0, cap)], rs.at[g], rr.at[g], g * TOP + x, tp
         )
 
     small = [
@@ -336,19 +359,7 @@
     nothing = jnp.zeros((2, rows), F32)
     wpieces[...] = jnp.concatenate(parts + [nothing], 0).astype(BF16)
 
-    loads[0].wait()
     strip = 32
-
-    def norm_rows(i, carry):
-        span = pl.ds(pl.multiple_of(i * strip, strip), strip)
-        wide_rows = tokens[span, :].astype(F32)
-        scale = lax.rsqrt(
-            jnp.sum(wide_rows * wide_rows, axis=1, keepdims=True) * (1.0 / width) + 1e-06
-        )
-        normal[span, :] = (wide_rows * scale * mgain_ref[...]).astype(BF16)
-        return carry
-
-    lax.fori_loop(0, rows // strip, norm_rows, 0)
 
     def halo_copy(t, e, c):
         cols = pl.ds(pl.multiple_of(c * chans, LANES), chans)
@@ -357,48 +368,70 @@
     loads[7].wait()
     loads[8].wait()
     edge[2] = (edge[0].astype(F32) * sigmoid(edge[1].astype(F32))).astype(BF16)
-    pl.semaphore_wait(barrier, expected)
-    for hop in hop_x:
-        hop.start()
-
-    @pl.when(ep < last_ep)
-    def _():
-        halo_copy(0, ep + 1, tp).start()
-
     zx = z + 1 - 2 * lax.rem(z, 2)
+    lo = z < 2
+    outer = jnp.logical_or(z == 0, z == 3)
+    across = jnp.where(lo, 2, 1)
+    far = jnp.where(lo, 3, 0)
+
+    def turn(k, table):
+        out = z
+        for place, (edge_peer, inner_peer) in enumerate(table):
+            for spot in range(GROUPS):
+                peer = (edge_peer, inner_peer, 3 - inner_peer, 3 - edge_peer)[spot]
+                out = jnp.where(jnp.logical_and(k == place, z == spot), peer, out)
+        return out
+
     block = 512
 
-    def dispatch(k, carry):
-        d = jnp.where(
-            k == 0, jnp.where(lo, 3, 0),
-            jnp.where(k == 1, zx, jnp.where(k == 2, jnp.where(lo, 2, 1), z)),
-        )
+    def fill(d):
         slot = slots[pl.ds(d, 1), :]
         pick = (
             lax.broadcasted_iota(jnp.int32, (wpad, rows), 0).astype(F32)
             == jnp.broadcast_to(slot, (wpad, rows))
         ).astype(F32).astype(BF16)
+        squares = jnp.zeros((cap, 1), F32)
+        for n in range(width // block):
+            cols = pl.ds(n * block, block)
+            chosen = jnp.dot(pick[:cap], tokens[:, cols], preferred_element_type=F32)
+            raw[:, cols] = chosen
+            squares = squares + jnp.sum(chosen * chosen, axis=1, keepdims=True)
         weights = lax.dot_general(
             wpieces[...], pick, (((1,), (1,)), ((), ())), preferred_element_type=F32
         )
+        wsend[d, 0:1, :] = weights[0:1] + weights[1:2] + weights[2:3]
+        wsend[d, 1:2, :] = weights[3:4] + weights[4:5] + weights[5:6]
+        scale = lax.rsqrt(squares * (1.0 / width) + 1e-06)
         for n in range(width // block):
             cols = pl.ds(n * block, block)
-            chosen = jnp.dot(pick[:cap], normal[:, cols], preferred_element_type=F32)
-            send[d, :, cols] = chosen.astype(BF16)
-        wsend[d] = weights
+            send[d, :, cols] = (raw[:, cols] * scale * mgain_ref[:, cols]).astype(BF16)
+
+    loads[0].wait()
+    start = turn(0, OUTWARD)
+    fill(start)
+    pl.semaphore_wait(barrier, expected)
+
+    @pl.when(ep < last_ep)
+    def _():
+        halo_copy(0, ep + 1, tp).start()
+
+    there(start).start()
+    weights_there(start).start()
+    for hop in hop_x:
+        hop.start()
+
+    def dispatch(k, carry):
+        d = turn(k, OUTWARD)
+        fill(d)
 
         @pl.when(k < 3)
         def _():
-            remote(
-                send.at[d], recv.at[z], zs.at[d], zr.at[z], d * TOP + x, tp
-            ).start()
-            remote(
-                wsend.at[d], wrecv.at[z], us.at[d], ur.at[z], d * TOP + x, tp
-            ).start()
+            there(d).start()
+            weights_there(d).start()
 
         return carry
 
-    lax.fori_loop(0, 4, dispatch, 0)
+    lax.fori_loop(1, 4, dispatch, 0)
     recv[z] = send[z]
     wrecv[z] = wsend[z]
 
@@ -513,23 +546,16 @@
     nb = 256
 
     def expert(i, carry):
-        even_z = lax.rem(z, 2) == 0
-        s = jnp.where(
-            i == 0, jnp.where(even_z, 3, 0),
-            jnp.where(
-                i == 1, lax.rem(z + 2, GROUPS),
-                jnp.where(i == 2, jnp.where(even_z, 1, 2), z),
-            ),
-        )
+        s = turn(i, HOMEWARD)
 
         @pl.when(i < 3)
         def _():
-            remote(send.at[s], recv.at[s], zs.at[s], zr.at[s], s * TOP + x, tp).wait_recv()
-            remote(wsend.at[s], wrecv.at[s], us.at[s], ur.at[s], s * TOP + x, tp).wait_recv()
+            here_from(s).wait_recv()
+            weights_here(s).wait_recv()
 
         w8 = wrecv[s]
-        w_low = w8[0:1] + w8[1:2] + w8[2:3]
-        w_high = w8[3:4] + w8[4:5] + w8[5:6]
+        w_low = w8[0:1]
+        w_high = w8[1:2]
         mine = jnp.where(even, w_low, w_high)
         theirs = jnp.where(even, w_high, w_low)
         mine = jnp.transpose(jnp.broadcast_to(mine, (LANES, wpad)))[:cap]
@@ -558,9 +584,7 @@
 
         @pl.when(i < 3)
         def _():
-            remote(
-                result.at[s], ret.at[z, pl.ds(0, cap)], rs.at[s], rr.at[z], s * TOP + x, tp
-            ).start()
+            back(s).start()
 
         return carry
 
@@ -592,14 +616,6 @@
             1,
         )
 
-    def returned(g):
-        return remote(
-            result.at[g], ret.at[g, pl.ds(0, cap)], rs.at[g], rr.at[g], g * TOP + x, tp
-        )
-
-    third = jnp.where(lo, 3, 0)
-    last = jnp.where(lo, 2, 1)
-
     def add_back(g, fresh):
         chosen = put(g)
         for n in range(width // nb):
@@ -613,7 +629,9 @@
     add_back(z, True)
 
     def rest(i, carry):
-        g = jnp.where(i == 0, zx, jnp.where(i == 1, third, last))
+        g = jnp.where(
+            i == 0, zx, jnp.where(jnp.logical_xor(outer, i == 1), far, across)
+        )
         returned(g).wait_recv()
         add_back(g, False)
         return carry
@@ -622,9 +640,9 @@
 
     for step in range(1, GROUPS):
         s = lax.rem(z + step, GROUPS)
-        remote(send.at[s], recv.at[s], zs.at[s], zr.at[s], s * TOP + x, tp).wait_send()
-        remote(wsend.at[s], wrecv.at[s], us.at[s], ur.at[s], s * TOP + x, tp).wait_send()
-        returned(s).wait_send()
+        there(s).wait_send()
+        weights_there(s).wait_send()
+        back(s).wait_send()
     for j in range(pieces):
         hop_x[j].wait_send()
         hop_y[j].wait_send()
@@ -684,13 +702,13 @@
             pltpu.VMEM((tile, all_chans), BF16),
             pltpu.VMEM((peers, chans, width), BF16),
             pltpu.VMEM((rows, width), BF16),
-            pltpu.VMEM((rows, width), BF16),
+            pltpu.VMEM((cap, width), F32),
             pltpu.VMEM((8, rows), F32),
             pltpu.VMEM((8, rows), BF16),
             pltpu.VMEM((GROUPS, cap, width), BF16),
             pltpu.VMEM((GROUPS, cap, width), BF16),
-            pltpu.VMEM((GROUPS, 8, wpad), F32),
-            pltpu.VMEM((GROUPS, 8, wpad), F32),
+            pltpu.VMEM((GROUPS, TOP, wpad), F32),
+            pltpu.VMEM((GROUPS, TOP, wpad), F32),
             pltpu.VMEM((width, ff), BF16),
             pltpu.VMEM((width, ff), BF16),
             pltpu.VMEM((ff, width), BF16),

time: 126 us -> 110 us (0.87)
  the two profiles are of different devices: /device:TPU:15 before, /device:TPU:8 now
where the time goes in v3:
time: 110 us
  Pallas kernels  107 us (97%)
  local copies, waits for them, and re-layouts  2.11 us (2%)
    pallas_call x1, Pallas kernels, one_kernel(): pl.pallas_call(functools.partial(fused, cap), out_shape=(jax.ShapeDtypeSt...  107 us

profile of v3, /device:TPU:8, one launch (start us, length us, event | category | flops | bytes accessed | tf_op | source)
XLA Modules:
  0.0 110.2 jit_solution(1493576138591100498)
XLA Ops:
  0.6 107.4 %fused.1 = (bf16[256,2048]{1,0:T(8,128)(2,1)S(1)}, bf16[384,2048]{1,0:T(8,128)(2,1)S(1)}) custom-call(bf16[1024,256]{1,0:T(8,128)(2,1)} %value_hbm.1, bf16[1024,256]{1,0:T(8,128)(2,1)} %gate_hbm.1, f32[31,1024]{1,0:T(8,128)} %taps_hbm.1, f32[1,1024]{1,0:T(1,128)} %bitcast.12, f32[1,1024]{1,0:T(1,128)} %bitcast.13, bf16[256,2048]{1,0:T(8,128)(2,1)} %wout_hbm.1, ...), custom_call_target="tpu_custom_call" | custom-call | tf_op jit(solution)/shard_map/fused/pallas_call | solution.py:679
  108.0 1.0 copy.17
  109.0 1.1 %copy.18 = bf16[384,2048]{1,0:T(8,128)(2,1)} copy(bf16[384,2048]{1,0:T(8,128)(2,1)S(1)} %get-tuple-element.5) | data formatting | bytes 3145728

commit v4 on v3

--- a/solution.py
+++ b/solution.py
@@ -223,25 +223,25 @@
         )
 
     def there(s):
-        return remote(send.at[s], recv.at[z], zs.at[s], zr.at[z], s * TOP + x, tp)
+        return remote(send.at[s], recv.at[z], zs, zr.at[z], s * TOP + x, tp)
 
     def here_from(s):
-        return remote(send.at[s], recv.at[s], zs.at[s], zr.at[s], s * TOP + x, tp)
+        return remote(send.at[s], recv.at[s], zs, zr.at[s], s * TOP + x, tp)
 
     def weights_there(s):
-        return remote(wsend.at[s], wrecv.at[z], us.at[s], ur.at[z], s * TOP + x, tp)
+        return remote(wsend.at[s], wrecv.at[z], us, ur.at[z], s * TOP + x, tp)
 
     def weights_here(s):
-        return remote(wsend.at[s], wrecv.at[s], us.at[s], ur.at[s], s * TOP + x, tp)
+        return remote(wsend.at[s], wrecv.at[s], us, ur.at[s], s * TOP + x, tp)
 
     def back(s):
         return remote(
-            result.at[s], ret.at[z, pl.ds(0, cap)], rs.at[s], rr.at[z], s * TOP + x, tp
+            result.at[s], ret.at[z, pl.ds(0, cap)], rs, rr.at[z], s * TOP + x, tp
         )
 
     def returned(g):
         return remote(
-            result.at[g], ret.at[g, pl.ds(0, cap)], rs.at[g], rr.at[g], g * TOP + x, tp
+            result.at[g], ret.at[g, pl.ds(0, cap)], rs, rr.at[g], g * TOP + x, tp
         )
 
     small = [
@@ -320,16 +320,19 @@
     hop_x = [
         remote(
             piece(j, tp, egate_hbm, eup_hbm, edown_hbm, False),
-            held(j, tp), xs.at[j], xr.at[j], z * TOP + 1 - x, tp,
+            held(j, tp), xs, xr.at[j], z * TOP + 1 - x, tp,
         )
         for j in range(pieces)
     ]
-    hop_y = [remote(held(j, tp), held(j, tp), ys.at[j], yr.at[j], ep, y_peer) for j in range(pieces)]
-    hop_d = [remote(held(j, tp), held(j, tp), ds.at[j], dr.at[j], ep, core_peer) for j in range(pieces)]
+    hop_y = [remote(held(j, tp), held(j, tp), ys, yr.at[j], ep, y_peer) for j in range(pieces)]
+    hop_d = [remote(held(j, tp), held(j, tp), ds, dr, ep, core_peer) for j in range(pieces)]
     hop_e = [
-        remote(held(j, y_peer), held(j, y_peer), es.at[j], er.at[j], ep, core_peer)
+        remote(held(j, y_peer), held(j, y_peer), es, er, ep, core_peer)
         for j in range(pieces)
     ]
+    quarter = pdown.at[pl.ds(0, 3 * share)]
+    whole_d = remote(quarter, quarter, ds, dr, ep, core_peer)
+    whole_e = remote(quarter, quarter, es, er, ep, core_peer)
 
     small[0].wait()
     small[1].wait()
@@ -363,7 +366,7 @@
 
     def halo_copy(t, e, c):
         cols = pl.ds(pl.multiple_of(c * chans, LANES), chans)
-        return remote(edge.at[2], halo.at[:, cols], hs, hr.at[c], e, t)
+        return remote(edge.at[2], halo.at[:, cols], hs, hr, e, t)
 
     loads[7].wait()
     loads[8].wait()
@@ -453,9 +456,11 @@
         return pl.ds(pl.multiple_of(t * tile, HALO), tile + HALO)
 
     gated_copies = [
-        remote(gpad.at[window(t)], gin.at[:, my_cols], gs.at[i], gr.at[i], ep, t)
-        for i, t in enumerate((core_peer, y_peer, diag))
+        remote(gpad.at[window(t)], gin.at[:, my_cols], gs, gr, ep, t)
+        for t in (core_peer, y_peer, diag)
     ]
+    three = gpad.at[pl.ds(0, 3 * (tile + HALO))]
+    whole_gated = remote(three, three, gs, gr, ep, core_peer)
     for copy in gated_copies:
         copy.start()
 
@@ -465,22 +470,20 @@
         ret[g, cap:, :] = jnp.zeros((ret.shape[1] - cap, width), BF16)
 
     own_wout = wout.at[tp]
-    out_y = remote(own_wout, own_wout, cs.at[0], cr.at[0], ep, y_peer)
-    out_d = remote(own_wout, own_wout, cs.at[1], cr.at[1], ep, core_peer)
-    out_e = remote(wout.at[y_peer], wout.at[y_peer], cs.at[2], cr.at[2], ep, core_peer)
+    out_y = remote(own_wout, own_wout, cs, cr.at[0], ep, y_peer)
+    out_d = remote(own_wout, own_wout, cs, cr.at[1], ep, core_peer)
+    out_e = remote(wout.at[y_peer], wout.at[y_peer], cs, cr.at[1], ep, core_peer)
 
     taps_count = taps_ref.shape[0]
     lane_blocks = gin.shape[1] // LANES
     frows = 64
 
     def widen():
-        for copy in gated_copies:
-            copy.wait_recv()
+        whole_gated.wait_recv()
 
         @pl.when(first_tp)
         def _():
-            for c in range(4):
-                halo_copy(0, ep, c).wait_recv()
+            remote(halo, halo, hs, hr, ep, core_peer).wait_recv()
             gin[0:HALO, :] = halo[...]
 
         for b in range(lane_blocks):
@@ -537,9 +540,8 @@
     hop_e[pieces - 1].start()
     for load in loads[3:6]:
         load.wait()
-    for j in range(pieces):
-        hop_d[j].wait_recv()
-        hop_e[j].wait_recv()
+    whole_d.wait_recv()
+    whole_e.wait_recv()
 
     ff = ogate.shape[1]
     even = x == 0
@@ -593,8 +595,8 @@
 
     out_y.wait_recv()
     out_e.start()
-    out_d.wait_recv()
-    out_e.wait_recv()
+    pair = wout.at[pl.ds(0, 2)]
+    remote(pair, pair, cs, cr.at[1], ep, core_peer).wait_recv()
 
     def project(n, carry):
         cols = pl.ds(pl.multiple_of(n * nb, nb), nb)
@@ -638,26 +640,33 @@
 
     lax.fori_loop(0, 3, rest, 0)
 
-    for step in range(1, GROUPS):
-        s = lax.rem(z + step, GROUPS)
-        there(s).wait_send()
-        weights_there(s).wait_send()
-        back(s).wait_send()
-    for j in range(pieces):
-        hop_x[j].wait_send()
-        hop_y[j].wait_send()
-        hop_d[j].wait_send()
-        hop_e[j].wait_send()
-    for copy in gated_copies:
-        copy.wait_send()
+    most = pl.ds(0, GROUPS - 1)
+    remote(send.at[most], recv.at[most], zs, zr.at[z], ep, core_peer).wait_send()
+    remote(wsend.at[most], wrecv.at[most], us, ur.at[z], ep, core_peer).wait_send()
+    remote(result.at[most], recv.at[most], rs, rr.at[z], ep, core_peer).wait_send()
+    remote(quarter, quarter, xs, xr.at[0], ep, core_peer).wait_send()
+    remote(quarter, quarter, ys, yr.at[0], ep, core_peer).wait_send()
+    whole_d.wait_send()
+    whole_e.wait_send()
+    whole_gated.wait_send()
 
     @pl.when(ep < last_ep)
     def _():
         halo_copy(0, ep + 1, tp).wait_send()
 
-    out_y.wait_send()
-    out_d.wait_send()
-    out_e.wait_send()
+    triple = wout.at[pl.ds(0, 3)]
+    remote(triple, triple, cs, cr.at[0], ep, core_peer).wait_send()
+
+
+def put_out(conv_ref, moe_ref, conv_hbm, moe_hbm, sems):
+    copies = (
+        pltpu.make_async_copy(conv_ref, conv_hbm, sems.at[0]),
+        pltpu.make_async_copy(moe_ref, moe_hbm, sems.at[1]),
+    )
+    for copy in copies:
+        copy.start()
+    for copy in copies:
+        copy.wait()
 
 
 def one_kernel(
@@ -676,7 +685,7 @@
     hbm = pl.BlockSpec(memory_space=pltpu.HBM)
     dma = pltpu.SemaphoreType.DMA
     blocks = all_chans // LANES
-    return pl.pallas_call(
+    outputs = pl.pallas_call(
         functools.partial(fused, cap),
         out_shape=(
             jax.ShapeDtypeStruct((tile, width), BF16),
@@ -718,16 +727,16 @@
             pltpu.VMEM((GROUPS, cap, width), BF16),
             pltpu.VMEM((GROUPS, wpad, width), BF16),
             dma((15,)),
-            dma((GROUPS,)), dma((GROUPS,)),
-            dma((GROUPS,)), dma((GROUPS,)),
-            dma((GROUPS,)), dma((GROUPS,)),
-            dma((6,)), dma((6,)),
-            dma((6,)), dma((6,)),
-            dma((6,)), dma((6,)),
-            dma((6,)), dma((6,)),
-            dma((3,)), dma((3,)),
-            dma(()), dma((4,)),
-            dma((3,)), dma((3,)),
+            dma(()), dma((GROUPS,)),
+            dma(()), dma((GROUPS,)),
+            dma(()), dma((GROUPS,)),
+            dma(()), dma((6,)),
+            dma(()), dma((6,)),
+            dma(()), dma(()),
+            dma(()), dma(()),
+            dma(()), dma(()),
+            dma(()), dma(()),
+            dma(()), dma((2,)),
         ],
         compiler_params=pltpu.CompilerParams(
             collective_id=0, has_side_effects=True, vmem_limit_bytes=46 * 1024 * 1024
@@ -743,6 +752,18 @@
             )
         )
     )
+    return pl.pallas_call(
+        put_out,
+        out_shape=(
+            jax.ShapeDtypeStruct((tile, width), BF16),
+            jax.ShapeDtypeStruct((rows, width), BF16),
+        ),
+        in_specs=[vmem, vmem],
+        out_specs=(hbm, hbm),
+        scratch_shapes=[dma((2,))],
+        compiler_params=pltpu.CompilerParams(vmem_limit_bytes=8 * 1024 * 1024),
+        name="put_out",
+    )(*outputs)
 
 
 def on_device(

time: 110 us -> 109 us (level)
  local copies, waits for them, and re-layouts: 2.11 us -> 0 us
    unnamed x2 -> x0, local copies, waits for them, and re-layouts: 2.11 us -> none
    pallas_call x0 -> x1, Pallas kernels: none -> 1.51 us  [one_kernel(): pl.pallas_call(put_out, out_shape=(jax.ShapeDtypeStruct((tile, width), BF...]
where the time goes in v4:
time: 109 us
  Pallas kernels  108 us (99%)
    pallas_call x1, Pallas kernels, one_kernel(): pl.pallas_call(functools.partial(fused, cap), out_shape=(jax.ShapeDtypeSt...  107 us

profile of v4, /device:TPU:8, one launch (start us, length us, event | category | flops | bytes accessed | tf_op | source)
XLA Modules:
  0.0 109.1 jit_solution(15835479808664404115)
XLA Ops:
  0.6 106.9 %fused.1 = (bf16[256,2048]{1,0:T(8,128)(2,1)S(1)}, bf16[384,2048]{1,0:T(8,128)(2,1)S(1)}) custom-call(bf16[1024,256]{1,0:T(8,128)(2,1)} %value_hbm.1, bf16[1024,256]{1,0:T(8,128)(2,1)} %gate_hbm.1, f32[31,1024]{1,0:T(8,128)} %taps_hbm.1, f32[1,1024]{1,0:T(1,128)} %bitcast.12, f32[1,1024]{1,0:T(1,128)} %bitcast.13, bf16[256,2048]{1,0:T(8,128)(2,1)} %wout_hbm.1, ...), custom_call_target="tpu_custom_call" | custom-call | tf_op jit(solution)/shard_map/fused/pallas_call | solution.py:688
  107.5 1.5 %put_out.1 = (bf16[256,2048]{1,0:T(8,128)(2,1)}, bf16[384,2048]{1,0:T(8,128)(2,1)}) custom-call(bf16[256,2048]{1,0:T(8,128)(2,1)S(1)} %get-tuple-element.4.conv_ref, bf16[384,2048]{1,0:T(8,128)(2,1)S(1)} %get-tuple-element.5.moe_ref), custom_call_target="tpu_custom_call" | custom-call | tf_op jit(solution)/shard_map/put_out/pallas_call | solution.py:755

commit v5 on v4

--- a/solution.py
+++ b/solution.py
@@ -143,6 +143,8 @@
     edown_hbm,
     conv_ref,
     moe_ref,
+    late_ref,
+    where_ref,
     taps_ref,
     gain_ref,
     shift_ref,
@@ -630,15 +632,19 @@
 
     add_back(z, True)
 
+    early = jnp.where(outer, across, far)
+    late = jnp.where(outer, far, across)
+    where_ref[...] = put(late)
+
     def rest(i, carry):
-        g = jnp.where(
-            i == 0, zx, jnp.where(jnp.logical_xor(outer, i == 1), far, across)
-        )
+        g = jnp.where(i == 0, zx, early)
         returned(g).wait_recv()
         add_back(g, False)
         return carry
 
-    lax.fori_loop(0, 3, rest, 0)
+    lax.fori_loop(0, 2, rest, 0)
+    returned(late).wait_recv()
+    late_ref[...] = ret[late]
 
     most = pl.ds(0, GROUPS - 1)
     remote(send.at[most], recv.at[most], zs, zr.at[z], ep, core_peer).wait_send()
@@ -658,13 +664,26 @@
     remote(triple, triple, cs, cr.at[0], ep, core_peer).wait_send()
 
 
-def put_out(conv_ref, moe_ref, conv_hbm, moe_hbm, sems):
-    copies = (
-        pltpu.make_async_copy(conv_ref, conv_hbm, sems.at[0]),
-        pltpu.make_async_copy(moe_ref, moe_hbm, sems.at[1]),
-    )
-    for copy in copies:
-        copy.start()
+def put_out(conv_ref, moe_ref, late_ref, where_ref, conv_hbm, moe_hbm, stage, sems):
+    block = 512
+    blocks = stage.shape[1] // block
+    conv_copy = pltpu.make_async_copy(conv_ref, conv_hbm, sems.at[blocks])
+    conv_copy.start()
+
+    def columns(n):
+        return pl.ds(n * block, block)
+
+    copies = [
+        pltpu.make_async_copy(stage.at[:, columns(n)], moe_hbm.at[:, columns(n)], sems.at[n])
+        for n in range(blocks)
+    ]
+    for n in range(blocks):
+        late = jnp.dot(where_ref[...], late_ref[:, columns(n)], preferred_element_type=F32)
+        stage[:, columns(n)] = (moe_ref[:, columns(n)].astype(F32) + late).astype(BF16)
+        if n > 0:
+            copies[n - 1].start()
+    copies[blocks - 1].start()
+    conv_copy.wait()
     for copy in copies:
         copy.wait()
 
@@ -690,9 +709,11 @@
         out_shape=(
             jax.ShapeDtypeStruct((tile, width), BF16),
             jax.ShapeDtypeStruct((rows, width), BF16),
+            jax.ShapeDtypeStruct((wpad, width), BF16),
+            jax.ShapeDtypeStruct((rows, wpad), BF16),
         ),
         in_specs=[hbm] * 13,
-        out_specs=(vmem, vmem),
+        out_specs=(vmem,) * 4,
         scratch_shapes=[
             pltpu.VMEM(depth_weight.shape, F32),
             pltpu.VMEM((1, all_chans), F32),
@@ -758,9 +779,9 @@
             jax.ShapeDtypeStruct((tile, width), BF16),
             jax.ShapeDtypeStruct((rows, width), BF16),
         ),
-        in_specs=[vmem, vmem],
+        in_specs=[vmem] * 4,
         out_specs=(hbm, hbm),
-        scratch_shapes=[dma((2,))],
+        scratch_shapes=[pltpu.VMEM((rows, width), BF16), dma((width // 512 + 1,))],
         compiler_params=pltpu.CompilerParams(vmem_limit_bytes=8 * 1024 * 1024),
         name="put_out",
     )(*outputs)

time: 109 us -> 109 us (level)
  no operation moved by 1% of the time
where the time goes in v5:
time: 109 us
  Pallas kernels  108 us (99%)
    pallas_call x1, Pallas kernels, one_kernel(): pl.pallas_call(functools.partial(fused, cap), out_shape=(jax.ShapeDtypeSt...  106 us

profile of v5, /device:TPU:8, one launch (start us, length us, event | category | flops | bytes accessed | tf_op | source)
XLA Modules:
  0.0 108.5 jit_solution(7297427337293360291)
XLA Ops:
  0.6 106.4 %fused.1 = (bf16[256,2048]{1,0:T(8,128)(2,1)S(1)}, bf16[384,2048]{1,0:T(8,128)(2,1)S(1)}, bf16[256,2048]{1,0:T(8,128)(2,1)S(1)}, bf16[384,256]{1,0:T(8,128)(2,1)S(1)}) custom-call(bf16[1024,256]{1,0:T(8,128)(2,1)} %value_hbm.1, bf16[1024,256]{1,0:T(8,128)(2,1)} %gate_hbm.1, f32[31,1024]{1,0:T(8,128)} %taps_hbm.1, f32[1,1024]{1,0:T(1,128)} %bitcast.12, ...), custom_call_target="tpu_custom_call" | custom-call | tf_op jit(solution)/shard_map/fused/pallas_call | solution.py:707
  107.0 1.6 %put_out.1 = (bf16[256,2048]{1,0:T(8,128)(2,1)}, bf16[384,2048]{1,0:T(8,128)(2,1)}) custom-call(bf16[256,2048]{1,0:T(8,128)(2,1)S(1)} %get-tuple-element.6.conv_ref, bf16[384,2048]{1,0:T(8,128)(2,1)S(1)} %get-tuple-element.7.moe_ref, bf16[256,2048]{1,0:T(8,128)(2,1)S(1)} %get-tuple-element.8.late_ref, bf16[384,256]{1,0:T(8,128)(2,1)S(1)} %get-tuple-element.9.where_ref), custom_call_target="tpu_custom_call" | custom-call | tf_op jit(solution)/shard_map/put_out/pallas_call | solution.py:776

commit v6 on v5

--- a/solution.py
+++ b/solution.py
@@ -635,6 +635,7 @@
     early = jnp.where(outer, across, far)
     late = jnp.where(outer, far, across)
     where_ref[...] = put(late)
+    late_ref[cap:, :] = jnp.zeros((ret.shape[1] - cap, width), BF16)
 
     def rest(i, carry):
         g = jnp.where(i == 0, zx, early)
@@ -644,7 +645,7 @@
 
     lax.fori_loop(0, 2, rest, 0)
     returned(late).wait_recv()
-    late_ref[...] = ret[late]
+    late_ref[0:cap, :] = ret[late, 0:cap, :]
 
     most = pl.ds(0, GROUPS - 1)
     remote(send.at[most], recv.at[most], zs, zr.at[z], ep, core_peer).wait_send()
@@ -679,7 +680,7 @@
     ]
     for n in range(blocks):
         late = jnp.dot(where_ref[...], late_ref[:, columns(n)], preferred_element_type=F32)
-        stage[:, columns(n)] = (moe_ref[:, columns(n)].astype(F32) + late).astype(BF16)
+        stage[:, columns(n)] = moe_ref[:, columns(n)] + late.astype(BF16)
         if n > 0:
             copies[n - 1].start()
     copies[blocks - 1].start()

time: 109 us -> 109 us (level)
  no operation moved by 1% of the time
where the time goes in v6:
time: 109 us
  Pallas kernels  108 us (99%)
    pallas_call x1, Pallas kernels, one_kernel(): pl.pallas_call(functools.partial(fused, cap), out_shape=(jax.ShapeDtypeSt...  106 us

profile of v6, /device:TPU:8, one launch (start us, length us, event | category | flops | bytes accessed | tf_op | source)
XLA Modules:
  0.0 108.5 jit_solution(3073963484807869576)
XLA Ops:
  0.6 106.3 %fused.1 = (bf16[256,2048]{1,0:T(8,128)(2,1)S(1)}, bf16[384,2048]{1,0:T(8,128)(2,1)S(1)}, bf16[256,2048]{1,0:T(8,128)(2,1)S(1)}, bf16[384,256]{1,0:T(8,128)(2,1)S(1)}) custom-call(bf16[1024,256]{1,0:T(8,128)(2,1)} %value_hbm.1, bf16[1024,256]{1,0:T(8,128)(2,1)} %gate_hbm.1, f32[31,1024]{1,0:T(8,128)} %taps_hbm.1, f32[1,1024]{1,0:T(1,128)} %bitcast.12, ...), custom_call_target="tpu_custom_call" | custom-call | tf_op jit(solution)/shard_map/fused/pallas_call | solution.py:708
  107.0 1.6 %put_out.1 = (bf16[256,2048]{1,0:T(8,128)(2,1)}, bf16[384,2048]{1,0:T(8,128)(2,1)}) custom-call(bf16[256,2048]{1,0:T(8,128)(2,1)S(1)} %get-tuple-element.6.conv_ref, bf16[384,2048]{1,0:T(8,128)(2,1)S(1)} %get-tuple-element.7.moe_ref, bf16[256,2048]{1,0:T(8,128)(2,1)S(1)} %get-tuple-element.8.late_ref, bf16[384,256]{1,0:T(8,128)(2,1)S(1)} %get-tuple-element.9.where_ref), custom_call_target="tpu_custom_call" | custom-call | tf_op jit(solution)/shard_map/put_out/pallas_call | solution.py:777

commit v7 on v6

--- a/solution.py
+++ b/solution.py
@@ -12,7 +12,7 @@
 LANES = 128
 HALO = 32
 MESH = pl.DeviceIdType.MESH
-OUTWARD = ((1, 3), (2, 0), (3, 2))
+OUTWARD = ((1, 3), (3, 2), (2, 0))
 HOMEWARD = ((3, 3), (1, 0), (2, 2))
 F32 = jnp.float32
 BF16 = jnp.bfloat16

time: 109 us -> 109 us (level)
  no operation moved by 1% of the time
where the time goes in v7:
time: 109 us
  Pallas kernels  108 us (99%)
    pallas_call x1, Pallas kernels, one_kernel(): pl.pallas_call(functools.partial(fused, cap), out_shape=(jax.ShapeDtypeSt...  106 us

profile of v7, /device:TPU:8, one launch (start us, length us, event | category | flops | bytes accessed | tf_op | source)
XLA Modules:
  0.0 108.5 jit_solution(2206523443849851308)
XLA Ops:
  0.6 106.3 %fused.1 = (bf16[256,2048]{1,0:T(8,128)(2,1)S(1)}, bf16[384,2048]{1,0:T(8,128)(2,1)S(1)}, bf16[256,2048]{1,0:T(8,128)(2,1)S(1)}, bf16[384,256]{1,0:T(8,128)(2,1)S(1)}) custom-call(bf16[1024,256]{1,0:T(8,128)(2,1)} %value_hbm.1, bf16[1024,256]{1,0:T(8,128)(2,1)} %gate_hbm.1, f32[31,1024]{1,0:T(8,128)} %taps_hbm.1, f32[1,1024]{1,0:T(1,128)} %bitcast.12, ...), custom_call_target="tpu_custom_call" | custom-call | tf_op jit(solution)/shard_map/fused/pallas_call | solution.py:708
  107.0 1.6 %put_out.1 = (bf16[256,2048]{1,0:T(8,128)(2,1)}, bf16[384,2048]{1,0:T(8,128)(2,1)}) custom-call(bf16[256,2048]{1,0:T(8,128)(2,1)S(1)} %get-tuple-element.6.conv_ref, bf16[384,2048]{1,0:T(8,128)(2,1)S(1)} %get-tuple-element.7.moe_ref, bf16[256,2048]{1,0:T(8,128)(2,1)S(1)} %get-tuple-element.8.late_ref, bf16[384,256]{1,0:T(8,128)(2,1)S(1)} %get-tuple-element.9.where_ref), custom_call_target="tpu_custom_call" | custom-call | tf_op jit(solution)/shard_map/put_out/pallas_call | solution.py:777
